TPU v7x, 256 devices: a whole 4x4x8 slice. The times are simulated.
256 devices in a mesh: fs: 32 (over z, y), tp: 8 (over x, core).
Axes of the slice: x: 4, y: 4, z: 8, core: 2. Of those that a mesh axis runs over, the one named last changes fastest.
Arguments:
- prompt: bfloat16 [24576, 2048], P('fs'), may hold values from -6 to 6
- routes: int32 [24576, 2], P('fs'), may hold values from 0 to 63, all different within a row; in each aligned block of 768 rows (0 to 767, 768 to 1535, ...) at most 48 rows name the same one
- affinity: float32 [24576, 2], P('fs'), may hold values from 0.05 to 1
- norm_gain: float32 [2048], P('fs'), may hold values from 0.1 to 1.9
- gate_master: float32 [64, 2048, 1024], P(None, 'fs', 'tp'), may hold values from -0.125 to 0.125
- up_master: float32 [64, 2048, 1024], P(None, 'fs', 'tp'), may hold values from -0.125 to 0.125
- down_master: float32 [64, 1024, 2048], P(None, 'fs', 'tp'), may hold values from -0.1875 to 0.1875
Outputs:
- mixed: bfloat16 [24576, 2048], P('fs', 'tp')
- gate_weights: bfloat16 [64, 2048, 1024], P('fs', None, 'tp')
- up_weights: bfloat16 [64, 2048, 1024], P('fs', None, 'tp')
- down_weights: bfloat16 [64, 1024, 2048], P('fs', None, 'tp')
Inputs may be any that keep to these rules, and one draw needn't show every extreme that they name: `routes`: each row names 2 different experts. In each aligned block of 768 rows no expert is named more than 48 times, a bound that some block reaches.
All inputs are finite; a program needn't handle non-finite values.
Results may differ from a plain program's by a relative error of at most 0.0086.
Values may be sent and summed in bfloat16 or wider, within the bound.
A program may use at most 128 MiB of HBM per device.

v0:
```python
import jax
import jax.numpy as jnp
from jax import lax
from jax.sharding import PartitionSpec as P

norm_eps = 1e-06


def side_by_side(arrays, axis, split_dim, concat_dim, along):
    widths = [a.shape[along] for a in arrays]
    both = jnp.concatenate(arrays, axis=along)
    whole = lax.all_to_all(both, axis, split_axis=split_dim, concat_axis=concat_dim, tiled=True)
    return tuple(jnp.split(whole, [sum(widths[:k]) for k in range(1, len(widths))], axis=along))


def per_device(prompt, routes, affinity, norm_gain, gate_master, up_master, down_master):
    tp_count = lax.axis_size("tp")
    experts = gate_master.shape[0]
    gain_rows = norm_gain[None, :, None]
    gate_half = (gate_master * gain_rows).astype(jnp.bfloat16)
    up_half = (up_master * gain_rows).astype(jnp.bfloat16)
    down_half = down_master.astype(jnp.bfloat16)
    gate_new, up_new, down_new = (
        *side_by_side((gate_half, up_half), "fs", 0, 1, 2),
        lax.all_to_all(down_half, "fs", split_axis=0, concat_axis=1, tiled=True),
    )
    token_count = prompt.shape[0]
    top_count = routes.shape[1]
    model_width = prompt.shape[1]
    capacity = 2 * token_count * top_count // experts
    flat_ids = routes.reshape(-1)
    onehot = (flat_ids[:, None] == jnp.arange(experts, dtype=jnp.int32)[None, :]).astype(jnp.int32)
    slot_rank = jnp.sum(jnp.cumsum(onehot, axis=0) * onehot, axis=1) - 1
    slot_index = flat_ids * capacity + slot_rank
    values = prompt.astype(jnp.float32)
    normed = (
        values * lax.rsqrt(jnp.mean(values * values, axis=-1, keepdims=True) + norm_eps)
    ).astype(jnp.bfloat16)
    column_width = model_width // tp_count
    column_slice = lax.dynamic_slice_in_dim(
        normed, lax.axis_index("tp") * column_width, column_width, 1
    )
    slot_rows = jnp.broadcast_to(
        column_slice[:, None, :], (token_count, top_count, column_width)
    ).reshape(-1, column_width)
    outbox = (
        jnp.zeros((experts * capacity, column_width), jnp.bfloat16).at[slot_index].set(slot_rows)
    )
    received = lax.all_to_all(
        outbox.reshape(experts, capacity, column_width),
        "fs",
        split_axis=0,
        concat_axis=1,
        tiled=True,
    )
    shard_piece = lax.all_gather(received, "tp", axis=2, tiled=True)
    gate_pre = jnp.einsum("erd,edf->erf", shard_piece, gate_new, preferred_element_type=jnp.float32)
    up_pre = jnp.einsum("erd,edf->erf", shard_piece, up_new, preferred_element_type=jnp.float32)
    hidden = (jax.nn.silu(gate_pre) * up_pre).astype(jnp.bfloat16)
    expert_out = jnp.einsum(
        "erf,efd->erd",
        lax.all_gather(hidden, "tp", axis=2, tiled=True),
        down_new,
        preferred_element_type=jnp.float32,
    ).astype(jnp.bfloat16)
    returned = lax.all_to_all(expert_out, "fs", split_axis=1, concat_axis=0, tiled=True)
    picked = returned.reshape(experts * capacity, -1)[slot_index].reshape(
        token_count, top_count, -1
    )
    share = affinity / jnp.sum(affinity, axis=1, keepdims=True)
    mixed_out = jnp.sum(share[:, :, None] * picked.astype(jnp.float32), axis=1).astype(jnp.bfloat16)
    return (mixed_out, gate_new, up_new, down_new)


def solution(mesh):
    in_specs = (
        P("fs", None),
        P("fs", None),
        P("fs", None),
        P("fs"),
        P(None, "fs", "tp"),
        P(None, "fs", "tp"),
        P(None, "fs", "tp"),
    )
    out_specs = (P("fs", "tp"), P("fs", None, "tp"), P("fs", None, "tp"), P("fs", None, "tp"))
    return jax.shard_map(
        per_device, mesh=mesh, in_specs=in_specs, out_specs=out_specs, check_vma=False
    )
```

profile of v0, /device:TPU:32, one launch (start us, length us, event | category | flops | bytes accessed | tf_op | source)
XLA Modules:
  0.0 309.4 jit_solution(14779207124408148616)
XLA Ops:
  7.2 5.5 %convert_element_type.36 = f32[768,2048]{1,0:T(8,128)} convert(bf16[768,2048]{1,0:T(8,128)(2,1)} %param.7) | non-fusion elementwise | flops 1572864 | bytes 9437184 | tf_op jit(solution)/shard_map/convert_element_type | solution.py:35
  12.8 0.7 multiply_reduce_fusion
  14.1 1.3 fusion.1
  15.5 0.4 broadcast_in_dim.5
  16.2 18.1 %reduce-window.6 = s32[64,12,128]{2,1,0:T(8,128)S(1)} reduce-window(s32[64,12,128]{2,1,0:T(8,128)S(1)} %fusion.4, s32[]{:T(128)} %constant.15.clone.1), window={size=1x1x128 pad=0_0x0_0x127_0}, to_apply=%region_1.2 | reduce-window | flops 12484608 | bytes 786436 | tf_op jit(solution)/shard_map/reduce-window
  35.8 7.6 %scatter_custom_fusion = bf16[3072,256]{1,0:T(8,128)(2,1)S(1)} fusion(s32[1536]{0:T(1024)S(1)} %fusion.7, bf16[1536,256]{1,0:T(8,128)(2,1)S(1)} %reshape.101, bf16[]{:T(256)} %constant.13.clone.1), kind=kCustom, calls=%fused_computation.12 | custom fusion | bytes 1572866 | tf_op jit(solution)/shard_map/scatter | solution.py:47
  43.5 50.9 %all_to_all.69 = bf16[64,48,256]{2,1,0:T(8,128)(2,1)S(1)} all-to-all(bf16[64,48,256]{2,1,0:T(8,128)(2,1)S(1)} %bitcast.43), channel_id=1, replica_groups=mesh['fs'=32,'tp'=8] {'fs'}, dimensions={0} | all-to-all | bytes 3145728 | tf_op jit(solution)/shard_map/all_to_all | solution.py:49
  94.4 1.3 copy.31
  95.7 0.8 copy-done.3
  96.5 2.2 multiply_convert_fusion.1
  99.0 54.0 %all_to_all.70 = bf16[64,64,256]{2,1,0:T(8,128)(2,1)S(1)} all-to-all(bf16[64,64,256]{2,1,0:T(8,128)(2,1)S(1)} %pad_maximum_fusion), channel_id=1, replica_groups=mesh['fs'=32,'tp'=8] {'fs'}, dimensions={0} | all-to-all | bytes 4194304 | tf_op jit(solution)/shard_map/all_to_all | solution.py:12
  153.7 12.7 %all-gather.3.cloned.1.call-done = bf16[2,1536,2048]{2,1,0:T(8,128)(2,1)} async-done(((bf16[2,1536,256]{2,1,0:T(8,128)(2,1)}), bf16[2,1536,2048]{2,1,0:T(8,128)(2,1)}) %all-gather.3.cloned.1.call-update) | async-done | bytes 12582928 | tf_op jit(solution)/shard_map/all_gather | solution.py:56
  166.4 7.8 %fusion.9 = f32[2,1536,128]{2,1,0:T(8,128)S(1)} fusion(bf16[2,1536,2048]{2,1,0:T(8,128)(2,1)} %all-gather.3.cloned.1.call-done, bf16[2,2048,128]{2,1,0:T(8,128)(2,1)S(1)} %get-tuple-element.4), kind=kOutput, calls=%fused_computation.29 | convolution fusion | flops 1610612736 | bytes 15204352 | tf_op jit(solution)/shard_map/erd,edf->erf/dot_general | solution.py:57
  174.1 0.4 copy-done.1
  174.5 4.7 %fusion = bf16[2,1536,128]{2,1,0:T(8,128)(2,1)} fusion(bf16[2,1536,2048]{2,1,0:T(8,128)(2,1)S(1)} %copy-done.1, bf16[2,2048,128]{2,1,0:T(8,128)(2,1)S(1)} %get-tuple-element.5, f32[2,1536,128]{2,1,0:T(8,128)S(1)} %fusion.9), kind=kOutput, calls=%fused_computation.5 | convolution fusion | flops 1612972032 | bytes 15990784 | tf_op jit(solution)/shard_map/erd,edf->erf/dot_general | solution.py:58
  179.4 37.5 %all_to_all.71 = bf16[64,32,256]{2,1,0:T(8,128)(2,1)S(1)} all-to-all(bf16[64,32,256]{2,1,0:T(8,128)(2,1)S(1)} %convert_element_type.41), channel_id=1, replica_groups=mesh['fs'=32,'tp'=8] {'fs'}, dimensions={0} | all-to-all | bytes 2097152 | tf_op jit(solution)/shard_map/all_to_all | solution.py:25
  217.0 10.4 %all-gather.5.cloned.1.call-done = bf16[2,1536,1024]{2,1,0:T(8,128)(2,1)} async-done(((bf16[2,1536,128]{2,1,0:T(8,128)(2,1)}), bf16[2,1536,1024]{2,1,0:T(8,128)(2,1)}) %all-gather.5.cloned.1.call-update) | async-done | bytes 6291472 | tf_op jit(solution)/shard_map/all_gather | solution.py:62
  227.3 4.6 %convolution_convert_fusion = bf16[2,1536,256]{2,1,0:T(8,128)(2,1)S(1)} fusion(bf16[2,1536,1024]{2,1,0:T(8,128)(2,1)} %all-gather.5.cloned.1.call-done, bf16[2,1024,256]{2,1,0:T(8,128)(2,1)S(1)} %bitcast.47), kind=kOutput, calls=%fused_computation.3 | convolution fusion | flops 1611399168 | bytes 8912896 | tf_op jit(solution)/shard_map/erf,efd->erd/dot_general | solution.py:60
  231.9 10.7 %copy.34 = bf16[2,1536,256]{2,0,1:T(2,128)(2,1)} copy(bf16[2,1536,256]{2,1,0:T(8,128)(2,1)S(1)} %convolution_convert_fusion) | data formatting | bytes 3145728 | tf_op jit(solution)/shard_map/convert_element_type | solution.py:65
  242.7 10.2 %all-to-all-start.3 = ((bf16[2,1536,256]{2,0,1:T(2,128)(2,1)}), bf16[2,1536,256]{2,0,1:T(2,128)(2,1)S(1)}, u32[]{:S(2)}, u32[]{:S(2)}) async-start(bf16[2,1536,256]{2,0,1:T(2,128)(2,1)} %copy.34), calls=%async_computation.3 | async-start | bytes 3145728 | tf_op jit(solution)/shard_map/all_to_all | solution.py:66
  253.2 38.6 %all-to-all-done.3 = bf16[2,1536,256]{2,0,1:T(2,128)(2,1)S(1)} async-done(((bf16[2,1536,256]{2,0,1:T(2,128)(2,1)}), bf16[2,1536,256]{2,0,1:T(2,128)(2,1)S(1)}, u32[]{:S(2)}, u32[]{:S(2)}) %all-to-all-start.3) | async-done | bytes 1572896 | tf_op jit(solution)/shard_map/all_to_all | solution.py:66
  292.0 4.8 %gather_fusion = bf16[1536,256]{1,0:T(8,128)(2,1)S(1)} fusion(bf16[3072,256]{1,0:T(8,128)(2,1)S(1)} %bitcast.38, s32[2048]{0:T(1024)S(1)} %pad_clamp_fusion), kind=kCustom, calls=%fused_computation | custom fusion | bytes 1579008 | tf_op jit(solution)/shard_map/gather | solution.py:67
  296.8 0.8 reshape.88
  297.5 5.0 %multiply_reduce_fusion.1 = bf16[768,256]{1,0:T(8,128)(2,1)} fusion(f32[768,2,256]{2,1,0:T(2,128)S(1)} %reshape.88, f32[768,2]{1,0:T(8,128)S(1)} %copy.25), kind=kLoop, calls=%fused_computation.9 | loop fusion | flops 589824 | bytes 1972224 | tf_op jit(solution)/shard_map/reduce_sum | solution.py:71
  (49 shorter events, 4.2 us)
Async XLA Ops:
  7.2 159.2 %all-gather.3.cloned.1.call-start = ((), (), s32[]{:S(2)}) async-start(), calls=%async_computation.4 | async-start | bytes 14155776 | tf_op jit(solution)/shard_map/all_gather | solution.py:56
  7.2 5.6 %copy-start = (bf16[768,2048]{1,0:T(8,128)(2,1)S(1)}, bf16[768,2048]{1,0:T(8,128)(2,1)}, u32[]{:S(2)}) copy-start(bf16[768,2048]{1,0:T(8,128)(2,1)} %param.7) | copy-start | bytes 9437188
  12.8 0.7 copy-start.8
  94.4 2.2 copy-start.3
  94.4 2.2 copy-start.9
  95.7 131.7 %all-gather.5.cloned.1.call-start = ((), (), s32[]{:S(2)}) async-start(), calls=%async_computation.5 | async-start | bytes 7077888 | tf_op jit(solution)/shard_map/all_gather | solution.py:62
  153.7 20.5 %copy-start.2 = (bf16[2,2048,128]{2,1,0:T(8,128)(2,1)}, bf16[2,2048,128]{2,1,0:T(8,128)(2,1)S(1)}, u32[]{:S(2)}) copy-start(bf16[2,2048,128]{2,1,0:T(8,128)(2,1)S(1)} %get-tuple-element.4) | copy-start | bytes 3145732
  153.7 20.5 %copy-start.6 = (bf16[2,2048,128]{2,1,0:T(8,128)(2,1)}, bf16[2,2048,128]{2,1,0:T(8,128)(2,1)S(1)}, u32[]{:S(2)}) copy-start(bf16[2,2048,128]{2,1,0:T(8,128)(2,1)S(1)} %get-tuple-element.5) | copy-start | bytes 3145732
  166.4 8.2 %copy-start.1 = (bf16[2,1536,2048]{2,1,0:T(8,128)(2,1)S(1)}, bf16[2,1536,2048]{2,1,0:T(8,128)(2,1)}, u32[]{:S(2)}) copy-start(bf16[2,1536,2048]{2,1,0:T(8,128)(2,1)} %all-gather.3.cloned.1.call-done) | copy-start | bytes 37748740
  174.5 4.7 %copy-start.4 = (f32[64,32,256]{2,1,0:T(8,128)S(1)}, f32[64,32,256]{2,1,0:T(8,128)}, u32[]{:S(2)}) copy-start(f32[64,32,256]{2,1,0:T(8,128)} %param.13) | copy-start | bytes 6291460
  217.0 15.0 %copy-start.5 = (bf16[32,2,32,256]{3,2,0,1:T(8,128)(2,1)}, bf16[32,2,32,256]{3,2,0,1:T(8,128)(2,1)S(1)}, u32[]{:S(2)}) copy-start(bf16[32,2,32,256]{3,2,0,1:T(8,128)(2,1)S(1)} %copy.33) | copy-start | bytes 3145732
  242.7 10.2 %copy-start.7 = (f32[768,2]{0,1:T(2,128)S(1)}, f32[768,2]{0,1:T(2,128)}, u32[]{:S(2)}) copy-start(f32[768,2]{0,1:T(2,128)} %param.9) | copy-start | bytes 18436
  242.7 49.1 %all-to-all-start.3 = ((bf16[2,1536,256]{2,0,1:T(2,128)(2,1)}), bf16[2,1536,256]{2,0,1:T(2,128)(2,1)S(1)}, u32[]{:S(2)}, u32[]{:S(2)}) async-start(bf16[2,1536,256]{2,0,1:T(2,128)(2,1)} %copy.34), calls=%async_computation.3 | async-start | bytes 3145728 | tf_op jit(solution)/shard_map/all_to_all | solution.py:66
Sparse Core Ops, SparseCore 0:
  95.8 70.5 all-gather.2
  179.4 47.9 all-gather.4
where the time goes:
time: 311 us; the launch traced here: 309 us
  blocking collectives  142 us (46%)
  waiting for transfers between devices  61.6 us (20%)
  other arithmetic  33.8 us (11%)
  local copies, waits for them, and re-layouts  29.9 us (10%)
  matrix products  17 us (5%)
  between operations  14.4 us (5%)
  starting transfers between devices  10.3 us (3%)
    all_to_all x1, blocking collectives, side_by_side(): lax.all_to_all(both, axis, split_axis=split_dim, concat_axis=concat_dim,...  54 us
    all_to_all x1, blocking collectives, per_device(): lax.all_to_all(outbox.reshape(experts, capacity, column_width), 'fs', spl...  50.9 us
    all_to_all x1, waiting for transfers between devices, per_device(): lax.all_to_all(expert_out, 'fs', split_axis=1, concat_axis=0, tiled=True)  38.6 us
    all_to_all x1, blocking collectives, per_device(): lax.all_to_all(down_half, 'fs', split_axis=0, concat_axis=1, tiled=True)  37.5 us
    another operation x3, other arithmetic  18.4 us
    all_gather x1, waiting for transfers between devices, per_device(): shard_piece = lax.all_gather(received, 'tp', axis=2, tiled=True)  12.7 us
    convert_element_type x1, local copies, waits for them, and re-layouts, per_device(): expert_out = jnp.einsum('erf,efd->erd', lax.all_gather(hidden, 'tp', axis...  10.7 us
    all_gather x1, waiting for transfers between devices, per_device(): lax.all_gather(hidden, 'tp', axis=2, tiled=True)  10.4 us
  transfers between devices with their start and end apart: 3, of which 3 were waited for; matrix products, arithmetic and copies ran while one was open for 1% of the time, Pallas kernels for 0%

commit v1 on v0

v1 whole, which is shorter than its diff:
```python
import jax
import jax.numpy as jnp
from jax import lax
from jax.experimental import pallas as pl
from jax.experimental.pallas import tpu as pltpu
from jax.sharding import PartitionSpec as P

MESH = pl.DeviceIdType.MESH
norm_eps = 1e-06

NZ, NY, NX = 8, 4, 4
NFS = NZ * NY
NTP = NX * 2
CAP = 48
BF16, F32 = jnp.bfloat16, jnp.float32


def plane_step(i):
    return 4 + ((i + 1) // 2) * (1 - 2 * (i % 2))


def loop(count, body):
    def step(i, carry):
        body(i)
        return carry

    lax.fori_loop(0, count, step, 0)


def kernel(
    rt_ref, at_ref, gain_ref, prompt_ref, gate_ref, up_ref, down_ref,
    mixed_ref, gate_out, up_out, down_out,
    pbuf, gbuf, ubuf, dbuf, wsend_gu, wsend_d, nm, outbox, tok, wgu, wd, hid, eo, ret, wcomb, macc,
    slots, load_sem, out_sem, swgu, swd, rwgu, rwd, st, sx, own, xl, xr, fl, fr, po, pl_, pr, pf,
    sh, hxl, hxr, hfl, hfr, hpo, hpl, hpr, hpf, sr, rr,
):
    me = lax.axis_index("fs")
    t = lax.axis_index("tp")
    mz, my = me // NY, me % NY
    mx, mc = t // 2, t % 2
    right = ((mx + 1) % NX) * 2 + mc
    left = ((mx + NX - 1) % NX) * 2 + mc
    far = ((mx + 2) % NX) * 2 + mc
    mate = mx * 2 + 1 - mc

    def load(n, src, dst):
        return pltpu.make_async_copy(src, dst, load_sem.at[n])

    loads = [
        load(0, gate_ref.at[:, 0], gbuf.at[0]),
        load(1, up_ref.at[:, 0], ubuf.at[0]),
        load(2, prompt_ref, pbuf),
        load(3, down_ref.at[:, 0], dbuf.at[0]),
        load(4, gate_ref.at[:, 1], gbuf.at[1]),
        load(5, up_ref.at[:, 1], ubuf.at[1]),
        load(6, down_ref.at[:, 1], dbuf.at[1]),
    ]
    for l in loads:
        l.start()

    barrier = pltpu.get_barrier_semaphore()

    def greet(i):
        pl.semaphore_signal(barrier, inc=1, device_id=((me + 1 + i) % NFS, t), device_id_type=MESH)

    loop(NFS - 1, greet)
    for other in (right, left, mate):
        pl.semaphore_signal(barrier, inc=1, device_id=(me, other), device_id_type=MESH)

    def remote(src, dst, ssem, rsem, fs, tp):
        return pltpu.make_async_remote_copy(
            src_ref=src, dst_ref=dst, send_sem=ssem, recv_sem=rsem, device_id=(fs, tp), device_id_type=MESH
        )

    def got(ref, sem):
        remote(ref, ref, sem, sem, me, t).wait_recv()

    def sent(ref, sem):
        remote(ref, ref, sem, sem, me, t).wait_send()

    def to_peers(send):
        def plane(i):
            z = (mz + plane_step(i)) % NZ
            for dy in range(NY):
                dst = z * NY + (my + dy) % NY
                if dy == 0:
                    @pl.when(i < NZ - 1)
                    def _():
                        send(dst)
                else:
                    send(dst)

        loop(NZ, plane)

    def cast_gu(e):
        loads[0 if e == 0 else 4].wait()
        loads[1 if e == 0 else 5].wait()

        def block(b):
            rows = pl.ds(b * 4, 4)
            gain = gain_ref[...][None]
            wsend_gu[e, rows, :, 0:128] = (gbuf[e, rows] * gain).astype(BF16)
            wsend_gu[e, rows, :, 128:256] = (ubuf[e, rows] * gain).astype(BF16)

        loop(8, block)
        wgu[e, pl.ds(pl.multiple_of(me * 64, 64), 64), :] = wsend_gu[e, me]

    def send_gu(e):
        def send(dst):
            remote(
                wsend_gu.at[e, dst], wgu.at[e, pl.ds(pl.multiple_of(me * 64, 64), 64)], swgu.at[e], rwgu.at[e], dst, t
            ).start()

        to_peers(send)

    def cast_d(e):
        loads[3 if e == 0 else 6].wait()

        def block(b):
            rows = pl.ds(b * 4, 4)
            wsend_d[e, rows] = dbuf[e, rows].astype(BF16)

        loop(8, block)
        wd[e, pl.ds(pl.multiple_of(me * 32, 32), 32), :] = wsend_d[e, me]

    def send_d(e):
        def send(dst):
            remote(
                wsend_d.at[e, dst], wd.at[e, pl.ds(pl.multiple_of(me * 32, 32), 32)], swd.at[e], rwd.at[e], dst, t
            ).start()

        to_peers(send)

    cast_gu(0)
    pl.semaphore_wait(barrier, NFS - 1 + 3)
    send_gu(0)

    r0, r1 = rt_ref[0:1, :], rt_ref[1:2, :]
    experts = lax.broadcasted_iota(jnp.int32, (64, 768), 0)
    oh0 = (experts == r0).astype(F32)
    oh1 = (experts == r1).astype(F32)
    before = lax.broadcasted_iota(jnp.int32, (768, 768), 0) < lax.broadcasted_iota(jnp.int32, (768, 768), 1)
    count = jnp.dot((oh0 + oh1).astype(BF16), before.astype(F32).astype(BF16), preferred_element_type=F32)
    rank0 = jnp.sum(count * oh0, axis=0, keepdims=True).astype(jnp.int32)
    rank1 = jnp.sum(count * oh1, axis=0, keepdims=True).astype(jnp.int32)
    slots[0:1, :] = r0 * CAP + rank0
    slots[1:2, :] = r1 * CAP + rank1

    loads[2].wait()

    def norm(b):
        rows = pl.ds(pl.multiple_of(b * 64, 64), 64)
        x = pbuf[rows, :].astype(F32)
        scale = lax.rsqrt(jnp.mean(x * x, axis=-1, keepdims=True) + norm_eps)
        mine = pbuf[rows, pl.ds(pl.multiple_of(t * 256, 256), 256)].astype(F32)
        nm[rows, :] = (mine * scale).astype(BF16)

    loop(12, norm)

    def build(i):
        z = (mz + plane_step(i)) % NZ
        index = lax.broadcasted_iota(jnp.int32, (8 * CAP, 768), 0) + z * (8 * CAP)
        hit = (index == slots[0:1, :]) | (index == slots[1:2, :])
        rows = jnp.dot(hit.astype(F32).astype(BF16), nm[...], preferred_element_type=F32)
        outbox[pl.ds(z * 8, 8)] = rows.astype(BF16).reshape(8, CAP, 256)

    def send_t(i):
        z = (mz + plane_step(i)) % NZ
        for dy in range(NY):
            dst = z * NY + (my + dy) % NY

            def go(dst=dst):
                remote(outbox.at[pl.ds(dst * 2, 2)], tok.at[t, me], st, own.at[i], dst, t).start()

            if dy == 0:
                pl.when(i < NZ - 1)(go)
            else:
                go()

    def dispatch(i):
        build(i)

        @pl.when(i > 0)
        def _():
            send_t(i - 1)

    loop(NZ, dispatch)
    tok[t, me] = outbox[pl.ds(me * 2, 2)]
    cast_d(0)
    send_t(NZ - 1)
    send_d(0)
    cast_gu(1)
    cast_d(1)
    send_gu(1)
    send_d(1)

    a0, a1 = at_ref[0:1, :], at_ref[1:2, :]
    total = a0 + a1

    def keys(r, rank, e):
        key = jnp.right_shift(r, 1) * CAP + rank
        return jnp.where(jnp.bitwise_and(r, 1) == e, key, -1).astype(F32)

    packed = jnp.concatenate(
        [keys(r0, rank0, 0), keys(r1, rank1, 0), keys(r0, rank0, 1), keys(r1, rank1, 1), a0 / total, a1 / total,
         jnp.zeros((122, 768), F32)],
        axis=0,
    )
    macc[...] = jnp.concatenate([packed.T, jnp.zeros((768, 128), F32)], axis=1)

    def weigh(b):
        rows = pl.ds(pl.multiple_of(b * 64, 64), 64)
        columns = macc[rows, 0:128]
        index = lax.broadcasted_iota(jnp.int32, (64, NFS * CAP), 1).astype(F32)
        for e in range(2):
            first = jnp.where(index == columns[:, 2 * e : 2 * e + 1], columns[:, 4:5], 0.0)
            second = jnp.where(index == columns[:, 2 * e + 1 : 2 * e + 2], columns[:, 5:6], 0.0)
            wcomb[e, rows, :] = (first + second).astype(BF16)

    loop(12, weigh)

    def plane_rows(i):
        z = (mz + NZ - plane_step(i)) % NZ
        return z * NY

    def gather(i):
        @pl.when(i < NZ)
        def _():
            at = plane_rows(i)

            @pl.when(i < NZ - 1)
            def _():
                got(tok.at[t, pl.ds(at, NY)], own.at[i])

            @pl.when(i == NZ - 1)
            def _():
                got(tok.at[t, pl.ds(at, NY - 1)], own.at[i])

            piece = tok.at[t, pl.ds(at, NY)]
            remote(piece, piece, sx, xl.at[i], me, right).start()
            remote(piece, piece, sx, xr.at[i], me, left).start()
            remote(piece, piece, sx, po.at[i], me, mate).start()

        @pl.when((i >= 1) & (i < NZ + 1))
        def _():
            j = i - 1
            at = plane_rows(j)
            whole = tok.at[left, pl.ds(at, NY)]
            half = tok.at[left, pl.ds(at, NY // 2)]
            got(whole, xl.at[j])
            remote(half, half, sx, fl.at[j], me, right).start()
            remote(whole, whole, sx, pl_.at[j], me, mate).start()
            whole = tok.at[right, pl.ds(at, NY)]
            half = tok.at[right, pl.ds(at + NY // 2, NY // 2)]
            got(whole, xr.at[j])
            remote(half, half, sx, fr.at[j], me, left).start()
            remote(whole, whole, sx, pr.at[j], me, mate).start()

        @pl.when(i >= 2)
        def _():
            j = i - 2
            at = plane_rows(j)
            whole = tok.at[far, pl.ds(at, NY)]
            got(tok.at[far, pl.ds(at, NY // 2)], fl.at[j])
            got(tok.at[far, pl.ds(at + NY // 2, NY // 2)], fr.at[j])
            remote(whole, whole, sx, pf.at[j], me, mate).start()

    loop(NZ + 2, gather)

    def gathered(i):
        at = pl.ds(plane_rows(i), NY)
        got(tok.at[mate, at], po.at[i])
        got(tok.at[left + 1 - 2 * mc, at], pl_.at[i])
        got(tok.at[right + 1 - 2 * mc, at], pr.at[i])
        got(tok.at[far + 1 - 2 * mc, at], pf.at[i])

    loop(NZ, gathered)

    CH = 8
    NCH = NFS // CH
    CR = CH * CAP

    def chunk_of(k):
        step = (2 + ((k + 1) // 2) * (1 - 2 * (k % 2))) % NCH
        return (mz // 2 + step) % NCH

    def expert(e):
        got(wsend_gu.at[e, pl.ds(0, NFS - 1)], rwgu.at[e])
        pltpu.make_async_copy(wgu.at[e, :, pl.ds(0, 128)], gate_out.at[e], out_sem.at[3 * e]).start()
        pltpu.make_async_copy(wgu.at[e, :, pl.ds(128, 128)], up_out.at[e], out_sem.at[3 * e + 1]).start()

        def hrows(k):
            return pl.ds(pl.multiple_of(chunk_of(k) * CR, CR), CR)

        def send_h(k):
            piece = hid.at[t, e, hrows(k)]
            remote(piece, piece, sh.at[e], hxl.at[e, k], me, right).start()
            remote(piece, piece, sh.at[e], hxr.at[e, k], me, left).start()
            remote(piece, piece, sh.at[e], hpo.at[e, k], me, mate).start()

        def forward_h(k):
            base = pl.multiple_of(chunk_of(k) * CR, CR)
            whole = hid.at[left, e, pl.ds(base, CR)]
            half = hid.at[left, e, pl.ds(base, CR // 2)]
            got(whole, hxl.at[e, k])
            remote(half, half, sh.at[e], hfl.at[e, k], me, right).start()
            remote(whole, whole, sh.at[e], hpl.at[e, k], me, mate).start()
            whole = hid.at[right, e, pl.ds(base, CR)]
            half = hid.at[right, e, pl.ds(base + CR // 2, CR // 2)]
            got(whole, hxr.at[e, k])
            remote(half, half, sh.at[e], hfr.at[e, k], me, left).start()
            remote(whole, whole, sh.at[e], hpr.at[e, k], me, mate).start()

        def pass_h(k):
            base = pl.multiple_of(chunk_of(k) * CR, CR)
            whole = hid.at[far, e, pl.ds(base, CR)]
            got(hid.at[far, e, pl.ds(base, CR // 2)], hfl.at[e, k])
            got(hid.at[far, e, pl.ds(base + CR // 2, CR // 2)], hfr.at[e, k])
            remote(whole, whole, sh.at[e], hpf.at[e, k], me, mate).start()

        def up_step(k):
            @pl.when(k < NCH)
            def _():
                senders = pl.ds(chunk_of(k) * CH, CH)
                acc = jnp.zeros((CR, 256), F32)
                for p in range(NTP):
                    x = tok[p, senders, e].reshape(CR, 256)
                    acc = acc + jnp.dot(x, wgu[e, p * 256 : (p + 1) * 256, :], preferred_element_type=F32)
                gate, up = acc[:, 0:128], acc[:, 128:256]
                hid[t, e, hrows(k), :] = (gate / (1.0 + jnp.exp(-gate)) * up).astype(BF16)

            @pl.when((k >= 1) & (k < NCH + 1))
            def _():
                send_h(k - 1)

            @pl.when((k >= 2) & (k < NCH + 2))
            def _():
                forward_h(k - 2)

            @pl.when(k >= 3)
            def _():
                pass_h(k - 3)

        loop(NCH + 3, up_step)

        got(wsend_d.at[e, pl.ds(0, NFS - 1)], rwd.at[e])
        pltpu.make_async_copy(wd.at[e], down_out.at[e], out_sem.at[3 * e + 2]).start()

        def send_r(k):
            plane = chunk_of(k) * 2
            for n in range(CH):
                s = (plane + n // NY) * NY + (my + n) % NY

                def go(s=s):
                    remote(eo.at[e, s], ret.at[e, me], sr.at[e], rr.at[e], s, t).start()

                if n % NY == 0:
                    pl.when(s != me)(go)
                else:
                    go()

        def down_step(k):
            @pl.when(k < NCH)
            def _():
                rows = hrows(k)
                got(hid.at[mate, e, rows], hpo.at[e, k])
                got(hid.at[left + 1 - 2 * mc, e, rows], hpl.at[e, k])
                got(hid.at[right + 1 - 2 * mc, e, rows], hpr.at[e, k])
                got(hid.at[far + 1 - 2 * mc, e, rows], hpf.at[e, k])
                acc = jnp.zeros((CR, 256), F32)
                for q in range(NX):
                    h = jnp.concatenate([hid[2 * q, e, rows, :], hid[2 * q + 1, e, rows, :]], axis=1)
                    acc = acc + jnp.dot(h, wd[e, q * 256 : (q + 1) * 256, :], preferred_element_type=F32)
                eo[e, pl.ds(chunk_of(k) * CH, CH)] = acc.astype(BF16).reshape(CH, CAP, 256)

            @pl.when(k >= 1)
            def _():
                send_r(k - 1)

        loop(NCH + 1, down_step)
        ret[e, me] = eo[e, me]

    expert(0)
    expert(1)

    got(ret.at[0, pl.ds(0, NFS - 1)], rr.at[0])

    def mix_first(b):
        rows = pl.ds(pl.multiple_of(b * 256, 256), 256)
        macc[rows, :] = jnp.dot(wcomb[0, rows, :], ret[0].reshape(NFS * CAP, 256), preferred_element_type=F32)

    loop(3, mix_first)
    got(ret.at[1, pl.ds(0, NFS - 1)], rr.at[1])

    def mix_second(b):
        rows = pl.ds(pl.multiple_of(b * 256, 256), 256)
        both = macc[rows, :] + jnp.dot(wcomb[1, rows, :], ret[1].reshape(NFS * CAP, 256), preferred_element_type=F32)
        mixed_ref[rows, :] = both.astype(BF16)

    loop(3, mix_second)

    for e in range(2):
        sent(wsend_gu.at[e, pl.ds(0, NFS - 1)], swgu.at[e])
        sent(wsend_d.at[e, pl.ds(0, NFS - 1)], swd.at[e])
        sent(hid.at[pl.ds(0, 7), e], sh.at[e])
        sent(eo.at[e, pl.ds(0, NFS - 1)], sr.at[e])
        pltpu.make_async_copy(wgu.at[e, :, pl.ds(0, 128)], gate_out.at[e], out_sem.at[3 * e]).wait()
        pltpu.make_async_copy(wgu.at[e, :, pl.ds(128, 128)], up_out.at[e], out_sem.at[3 * e + 1]).wait()
        pltpu.make_async_copy(wd.at[e], down_out.at[e], out_sem.at[3 * e + 2]).wait()
    sent(outbox.at[pl.ds(0, 2 * (NFS - 1))], st)
    sent(tok.at[pl.ds(0, 7)], sx)


def per_device(prompt, routes, affinity, norm_gain, gate_master, up_master, down_master):
    vmem = pl.BlockSpec(memory_space=pltpu.VMEM)
    hbm = pl.BlockSpec(memory_space=pl.ANY)
    dma = pltpu.SemaphoreType.DMA
    scratch = [
        pltpu.VMEM((768, 2048), BF16),
        pltpu.VMEM((2, 32, 64, 128), F32),
        pltpu.VMEM((2, 32, 64, 128), F32),
        pltpu.VMEM((2, 32, 32, 256), F32),
        pltpu.VMEM((2, 32, 64, 256), BF16),
        pltpu.VMEM((2, 32, 32, 256), BF16),
        pltpu.VMEM((768, 256), BF16),
        pltpu.VMEM((64, CAP, 256), BF16),
        pltpu.VMEM((NTP, NFS, 2, CAP, 256), BF16),
        pltpu.VMEM((2, 2048, 256), BF16),
        pltpu.VMEM((2, 1024, 256), BF16),
        pltpu.VMEM((NTP, 2, NFS * CAP, 128), BF16),
        pltpu.VMEM((2, NFS, CAP, 256), BF16),
        pltpu.VMEM((2, NFS, CAP, 256), BF16),
        pltpu.VMEM((2, 768, NFS * CAP), BF16),
        pltpu.VMEM((768, 256), F32),
        pltpu.VMEM((8, 768), jnp.int32),
        dma((7,)),
        dma((6,)),
        dma((2,)), dma((2,)), dma((2,)), dma((2,)),
        dma, dma,
        *[dma((NZ,)) for _ in range(9)],
        dma((2,)),
        *[dma((2, 4)) for _ in range(8)],
        dma((2,)), dma((2,)),
    ]
    return pl.pallas_call(
        kernel,
        out_shape=(
            jax.ShapeDtypeStruct((768, 256), BF16),
            jax.ShapeDtypeStruct((2, 2048, 128), BF16),
            jax.ShapeDtypeStruct((2, 2048, 128), BF16),
            jax.ShapeDtypeStruct((2, 1024, 256), BF16),
        ),
        in_specs=[vmem] * 3 + [hbm] * 4,
        out_specs=(vmem, hbm, hbm, hbm),
        scratch_shapes=scratch,
        compiler_params=pltpu.CompilerParams(
            collective_id=0, has_side_effects=True, vmem_limit_bytes=60 * 1024 * 1024
        ),
        name="hand_off",
    )(
        routes.T,
        affinity.T,
        jnp.broadcast_to(norm_gain[:, None], (64, 128)),
        prompt,
        gate_master.reshape(32, 2, 64, 128),
        up_master.reshape(32, 2, 64, 128),
        down_master.reshape(32, 2, 32, 256),
    )


def solution(mesh):
    in_specs = (
        P("fs", None),
        P("fs", None),
        P("fs", None),
        P("fs"),
        P(None, "fs", "tp"),
        P(None, "fs", "tp"),
        P(None, "fs", "tp"),
    )
    out_specs = (P("fs", "tp"), P("fs", None, "tp"), P("fs", None, "tp"), P("fs", None, "tp"))
    return jax.shard_map(
        per_device, mesh=mesh, in_specs=in_specs, out_specs=out_specs, check_vma=False
    )
```

time: 311 us -> 175 us (0.56)
  Pallas kernels: 0 us -> 167 us
  blocking collectives: 142 us -> 0 us
  waiting for transfers between devices: 61.6 us -> 0 us
  other arithmetic: 33.8 us -> 0 us
  local copies, waits for them, and re-layouts: 29.9 us -> 7.5 us
  matrix products: 17 us -> 0 us
  between operations: 14.4 us -> 0.65 us
  starting transfers between devices: 10.3 us -> 0 us
    pallas_call x0 -> x1, Pallas kernels: none -> 167 us  [per_device(): pl.pallas_call(kernel, out_shape=(jax.ShapeDtypeStruct((768, 256), BF16),...]
    all_to_all x3 -> x0, blocking collectives: 142 us -> none  [the longest x1 54 us: side_by_side(): lax.all_to_all(both, axis, split_axis=split_dim, concat_axis=concat_dim,...]
    all_to_all x1 -> x0, waiting for transfers between devices: 38.6 us -> none  [per_device(): lax.all_to_all(expert_out, 'fs', split_axis=1, concat_axis=0, tiled=True)]
    all_gather x2 -> x0, waiting for transfers between devices: 23 us -> none  [the longest x1 12.7 us: per_device(): shard_piece = lax.all_gather(received, 'tp', axis=2, tiled=True)]
    another operation x3 -> x0, other arithmetic: 18.4 us -> none
    dot_general x3 -> x0, matrix products: 17 us -> none  [the longest x1 7.76 us: per_device(): jnp.einsum('erd,edf->erf', shard_piece, gate_new, preferred_element_type=...]
    convert_element_type x2 -> x0, local copies, waits for them, and re-layouts: 11.5 us -> none  [the longest x1 10.7 us: per_device(): expert_out = jnp.einsum('erf,efd->erd', lax.all_gather(hidden, 'tp', axis...]
    all_to_all x1 -> x0, starting transfers between devices: 10.2 us -> none  [per_device(): lax.all_to_all(expert_out, 'fs', split_axis=1, concat_axis=0, tiled=True)]
  transfers between devices with their start and end apart: 3 -> 0, of which waited for: 3 -> 0; matrix products, arithmetic and copies ran while one was open for 1% -> 0% of each run, Pallas kernels for 0% -> 0%
where the time goes in v1:
time: 175 us
  Pallas kernels  167 us (95%)
  local copies, waits for them, and re-layouts  7.5 us (4%)
    pallas_call x1, Pallas kernels, per_device(): pl.pallas_call(kernel, out_shape=(jax.ShapeDtypeStruct((768, 256), BF16),...  167 us
    unnamed x8, local copies, waits for them, and re-layouts  6.15 us

profile of v1, /device:TPU:32, one launch (start us, length us, event | category | flops | bytes accessed | tf_op | source)
XLA Modules:
  0.0 175.2 jit_solution(15279200099569807571)
XLA Ops:
  0.6 1.3 broadcast_in_dim.2.gain_ref
  2.0 167.1 %hand_off.1 = (bf16[768,256]{1,0:T(8,128)(2,1)}, bf16[2,2048,128]{2,1,0:T(8,128)(2,1)}, bf16[2,2048,128]{2,1,0:T(8,128)(2,1)}, bf16[2,1024,256]{2,1,0:T(8,128)(2,1)}) custom-call(s32[2,768]{1,0:T(2,128)} %bitcast.8, f32[2,768]{1,0:T(2,128)} %bitcast.9, f32[64,128]{1,0:T(8,128)} %broadcast_in_dim.2.gain_ref, bf16[768,2048]{1,0:T(8,128)(2,1)} %prompt_ref.1, ...), custom_call_target="tpu_custom_call" | custom-call | tf_op jit(solution)/shard_map/hand_off/pallas_call | solution.py:445
  169.1 0.0 copy-start.1
  169.1 1.9 %copy.15 = bf16[768,256]{1,0:T(8,128)(2,1)} copy(bf16[768,256]{1,0:T(8,128)(2,1)} %get-tuple-element.8) | data formatting | bytes 786432
  170.9 0.0 copy-start
  170.9 2.4 %copy.16 = bf16[2,2048,128]{2,1,0:T(8,128)(2,1)} copy(bf16[2,2048,128]{2,1,0:T(8,128)(2,1)} %get-tuple-element.9) | data formatting | bytes 2097152
  173.3 0.0 copy-done.1
  173.3 1.0 copy.17
  174.2 0.0 copy-done
  174.3 1.0 copy.18
Async XLA Ops:
  169.1 4.2 %copy-start.1 = (bf16[2,2048,128]{2,1,0:T(8,128)(2,1)S(1)}, bf16[2,2048,128]{2,1,0:T(8,128)(2,1)}, u32[]{:S(2)}) copy-start(bf16[2,2048,128]{2,1,0:T(8,128)(2,1)} %get-tuple-element.10) | copy-start | bytes 3145732
  170.9 3.3 %copy-start = (bf16[2,1024,256]{2,1,0:T(8,128)(2,1)S(1)}, bf16[2,1024,256]{2,1,0:T(8,128)(2,1)}, u32[]{:S(2)}) copy-start(bf16[2,1024,256]{2,1,0:T(8,128)(2,1)} %get-tuple-element.11) | copy-start | bytes 3145732

commit v2 on v1

--- a/solution.py
+++ b/solution.py
@@ -16,7 +16,7 @@
 
 
 def plane_step(i):
-    return 4 + ((i + 1) // 2) * (1 - 2 * (i % 2))
+    return NZ + ((i + 1) // 2) * (2 * (i % 2) - 1)
 
 
 def loop(count, body):
@@ -47,10 +47,10 @@
         return pltpu.make_async_copy(src, dst, load_sem.at[n])
 
     loads = [
+        load(3, down_ref.at[:, 0], dbuf.at[0]),
+        load(2, prompt_ref, pbuf),
         load(0, gate_ref.at[:, 0], gbuf.at[0]),
         load(1, up_ref.at[:, 0], ubuf.at[0]),
-        load(2, prompt_ref, pbuf),
-        load(3, down_ref.at[:, 0], dbuf.at[0]),
         load(4, gate_ref.at[:, 1], gbuf.at[1]),
         load(5, up_ref.at[:, 1], ubuf.at[1]),
         load(6, down_ref.at[:, 1], dbuf.at[1]),
@@ -84,7 +84,7 @@
             for dy in range(NY):
                 dst = z * NY + (my + dy) % NY
                 if dy == 0:
-                    @pl.when(i < NZ - 1)
+                    @pl.when(i > 0)
                     def _():
                         send(dst)
                 else:
@@ -93,8 +93,8 @@
         loop(NZ, plane)
 
     def cast_gu(e):
-        loads[0 if e == 0 else 4].wait()
-        loads[1 if e == 0 else 5].wait()
+        loads[2 if e == 0 else 4].wait()
+        loads[3 if e == 0 else 5].wait()
 
         def block(b):
             rows = pl.ds(b * 4, 4)
@@ -114,7 +114,7 @@
         to_peers(send)
 
     def cast_d(e):
-        loads[3 if e == 0 else 6].wait()
+        loads[0 if e == 0 else 6].wait()
 
         def block(b):
             rows = pl.ds(b * 4, 4)
@@ -131,9 +131,9 @@
 
         to_peers(send)
 
-    cast_gu(0)
+    cast_d(0)
     pl.semaphore_wait(barrier, NFS - 1 + 3)
-    send_gu(0)
+    send_d(0)
 
     r0, r1 = rt_ref[0:1, :], rt_ref[1:2, :]
     experts = lax.broadcasted_iota(jnp.int32, (64, 768), 0)
@@ -146,7 +146,7 @@
     slots[0:1, :] = r0 * CAP + rank0
     slots[1:2, :] = r1 * CAP + rank1
 
-    loads[2].wait()
+    loads[1].wait()
 
     def norm(b):
         rows = pl.ds(pl.multiple_of(b * 64, 64), 64)
@@ -173,7 +173,7 @@
                 remote(outbox.at[pl.ds(dst * 2, 2)], tok.at[t, me], st, own.at[i], dst, t).start()
 
             if dy == 0:
-                pl.when(i < NZ - 1)(go)
+                pl.when(i > 0)(go)
             else:
                 go()
 
@@ -186,41 +186,16 @@
 
     loop(NZ, dispatch)
     tok[t, me] = outbox[pl.ds(me * 2, 2)]
-    cast_d(0)
+    cast_gu(0)
     send_t(NZ - 1)
-    send_d(0)
+    send_gu(0)
     cast_gu(1)
     cast_d(1)
     send_gu(1)
     send_d(1)
 
-    a0, a1 = at_ref[0:1, :], at_ref[1:2, :]
-    total = a0 + a1
-
-    def keys(r, rank, e):
-        key = jnp.right_shift(r, 1) * CAP + rank
-        return jnp.where(jnp.bitwise_and(r, 1) == e, key, -1).astype(F32)
-
-    packed = jnp.concatenate(
-        [keys(r0, rank0, 0), keys(r1, rank1, 0), keys(r0, rank0, 1), keys(r1, rank1, 1), a0 / total, a1 / total,
-         jnp.zeros((122, 768), F32)],
-        axis=0,
-    )
-    macc[...] = jnp.concatenate([packed.T, jnp.zeros((768, 128), F32)], axis=1)
-
-    def weigh(b):
-        rows = pl.ds(pl.multiple_of(b * 64, 64), 64)
-        columns = macc[rows, 0:128]
-        index = lax.broadcasted_iota(jnp.int32, (64, NFS * CAP), 1).astype(F32)
-        for e in range(2):
-            first = jnp.where(index == columns[:, 2 * e : 2 * e + 1], columns[:, 4:5], 0.0)
-            second = jnp.where(index == columns[:, 2 * e + 1 : 2 * e + 2], columns[:, 5:6], 0.0)
-            wcomb[e, rows, :] = (first + second).astype(BF16)
-
-    loop(12, weigh)
-
     def plane_rows(i):
-        z = (mz + NZ - plane_step(i)) % NZ
+        z = (mz + 2 * NZ - plane_step(i)) % NZ
         return z * NY
 
     def gather(i):
@@ -228,11 +203,11 @@
         def _():
             at = plane_rows(i)
 
-            @pl.when(i < NZ - 1)
+            @pl.when(i > 0)
             def _():
                 got(tok.at[t, pl.ds(at, NY)], own.at[i])
 
-            @pl.when(i == NZ - 1)
+            @pl.when(i == 0)
             def _():
                 got(tok.at[t, pl.ds(at, NY - 1)], own.at[i])
 
@@ -382,6 +357,33 @@
 
     expert(0)
     expert(1)
+
+    r0, r1 = rt_ref[0:1, :], rt_ref[1:2, :]
+    rank0, rank1 = slots[0:1, :] - r0 * CAP, slots[1:2, :] - r1 * CAP
+    a0, a1 = at_ref[0:1, :], at_ref[1:2, :]
+    total = a0 + a1
+
+    def keys(r, rank, e):
+        key = jnp.right_shift(r, 1) * CAP + rank
+        return jnp.where(jnp.bitwise_and(r, 1) == e, key, -1).astype(F32)
+
+    packed = jnp.concatenate(
+        [keys(r0, rank0, 0), keys(r1, rank1, 0), keys(r0, rank0, 1), keys(r1, rank1, 1), a0 / total, a1 / total,
+         jnp.zeros((122, 768), F32)],
+        axis=0,
+    )
+    macc[...] = jnp.concatenate([packed.T, jnp.zeros((768, 128), F32)], axis=1)
+
+    def weigh(b):
+        rows = pl.ds(pl.multiple_of(b * 64, 64), 64)
+        columns = macc[rows, 0:128]
+        index = lax.broadcasted_iota(jnp.int32, (64, NFS * CAP), 1).astype(F32)
+        for e in range(2):
+            first = jnp.where(index == columns[:, 2 * e : 2 * e + 1], columns[:, 4:5], 0.0)
+            second = jnp.where(index == columns[:, 2 * e + 1 : 2 * e + 2], columns[:, 5:6], 0.0)
+            wcomb[e, rows, :] = (first + second).astype(BF16)
+
+    loop(12, weigh)
 
     got(ret.at[0, pl.ds(0, NFS - 1)], rr.at[0])
 

time: 175 us -> 159 us (0.909)
  Pallas kernels: 167 us -> 150 us
    pallas_call x1, Pallas kernels: 167 us -> 150 us  [per_device(): pl.pallas_call(kernel, out_shape=(jax.ShapeDtypeStruct((768, 256), BF16),...]
where the time goes in v2:
time: 159 us
  Pallas kernels  150 us (94%)
  local copies, waits for them, and re-layouts  7.5 us (5%)
    pallas_call x1, Pallas kernels, per_device(): pl.pallas_call(kernel, out_shape=(jax.ShapeDtypeStruct((768, 256), BF16),...  150 us
    unnamed x8, local copies, waits for them, and re-layouts  6.15 us

profile of v2, /device:TPU:32, one launch (start us, length us, event | category | flops | bytes accessed | tf_op | source)
XLA Modules:
  0.0 158.5 jit_solution(4923856496844317523)
XLA Ops:
  0.6 1.3 broadcast_in_dim.2.gain_ref
  2.0 150.4 %hand_off.1 = (bf16[768,256]{1,0:T(8,128)(2,1)}, bf16[2,2048,128]{2,1,0:T(8,128)(2,1)}, bf16[2,2048,128]{2,1,0:T(8,128)(2,1)}, bf16[2,1024,256]{2,1,0:T(8,128)(2,1)}) custom-call(s32[2,768]{1,0:T(2,128)} %bitcast.8, f32[2,768]{1,0:T(2,128)} %bitcast.9, f32[64,128]{1,0:T(8,128)} %broadcast_in_dim.2.gain_ref, bf16[768,2048]{1,0:T(8,128)(2,1)} %prompt_ref.1, ...), custom_call_target="tpu_custom_call" | custom-call | tf_op jit(solution)/shard_map/hand_off/pallas_call | solution.py:447
  152.3 0.0 copy-start.1
  152.4 1.9 %copy.15 = bf16[768,256]{1,0:T(8,128)(2,1)} copy(bf16[768,256]{1,0:T(8,128)(2,1)} %get-tuple-element.8) | data formatting | bytes 786432
  154.2 0.0 copy-start
  154.2 2.4 %copy.16 = bf16[2,2048,128]{2,1,0:T(8,128)(2,1)} copy(bf16[2,2048,128]{2,1,0:T(8,128)(2,1)} %get-tuple-element.9) | data formatting | bytes 2097152
  156.6 0.0 copy-done.1
  156.6 1.0 copy.17
  157.5 0.0 copy-done
  157.5 1.0 copy.18
Async XLA Ops:
  152.3 4.2 %copy-start.1 = (bf16[2,2048,128]{2,1,0:T(8,128)(2,1)S(1)}, bf16[2,2048,128]{2,1,0:T(8,128)(2,1)}, u32[]{:S(2)}) copy-start(bf16[2,2048,128]{2,1,0:T(8,128)(2,1)} %get-tuple-element.10) | copy-start | bytes 3145732
  154.2 3.3 %copy-start = (bf16[2,1024,256]{2,1,0:T(8,128)(2,1)S(1)}, bf16[2,1024,256]{2,1,0:T(8,128)(2,1)}, u32[]{:S(2)}) copy-start(bf16[2,1024,256]{2,1,0:T(8,128)(2,1)} %get-tuple-element.11) | copy-start | bytes 3145732

commit v3 on v2

--- a/solution.py
+++ b/solution.py
@@ -28,10 +28,10 @@
 
 
 def kernel(
-    rt_ref, at_ref, gain_ref, prompt_ref, gate_ref, up_ref, down_ref,
-    mixed_ref, gate_out, up_out, down_out,
-    pbuf, gbuf, ubuf, dbuf, wsend_gu, wsend_d, nm, outbox, tok, wgu, wd, hid, eo, ret, wcomb, macc,
-    slots, load_sem, out_sem, swgu, swd, rwgu, rwd, st, sx, own, xl, xr, fl, fr, po, pl_, pr, pf,
+    rt_hbm, at_hbm, gain_hbm, prompt_ref, gate_ref, up_ref, down_ref,
+    wgu, wd, macc, wcomb1, ret1,
+    rt_ref, at_ref, gain_ref, pbuf, gbuf, ubuf, dbuf, wsend_gu, wsend_d, nm, outbox, tok, hid, eo, ret0, wcomb0,
+    slots, load_sem, swgu, swd, rwgu, rwd, st, sx, own, xl, xr, fl, fr, po, pl_, pr, pf,
     sh, hxl, hxr, hfl, hfr, hpo, hpl, hpr, hpf, sr, rr,
 ):
     me = lax.axis_index("fs")
@@ -43,6 +43,8 @@
     far = ((mx + 2) % NX) * 2 + mc
     mate = mx * 2 + 1 - mc
 
+    ret, wcomb = (ret0, ret1), (wcomb0, wcomb1)
+
     def load(n, src, dst):
         return pltpu.make_async_copy(src, dst, load_sem.at[n])
 
@@ -54,9 +56,12 @@
         load(4, gate_ref.at[:, 1], gbuf.at[1]),
         load(5, up_ref.at[:, 1], ubuf.at[1]),
         load(6, down_ref.at[:, 1], dbuf.at[1]),
+        load(7, rt_hbm, rt_ref),
+        load(8, at_hbm, at_ref),
+        load(9, gain_hbm, gain_ref),
     ]
-    for l in loads:
-        l.start()
+    for n in (0, 7, 1, 9, 2, 3, 4, 5, 6, 8):
+        loads[n].start()
 
     barrier = pltpu.get_barrier_semaphore()
 
@@ -93,12 +98,17 @@
         loop(NZ, plane)
 
     def cast_gu(e):
+        if e == 0:
+            loads[9].wait()
         loads[2 if e == 0 else 4].wait()
         loads[3 if e == 0 else 5].wait()
 
+        diagonal = lax.broadcasted_iota(jnp.int32, (64, 64), 0) == lax.broadcasted_iota(jnp.int32, (64, 64), 1)
+        column = jnp.sum(jnp.where(diagonal, gain_ref[...], 0.0), axis=1, keepdims=True)
+        gain = jnp.broadcast_to(column, (64, 128))[None]
+
         def block(b):
             rows = pl.ds(b * 4, 4)
-            gain = gain_ref[...][None]
             wsend_gu[e, rows, :, 0:128] = (gbuf[e, rows] * gain).astype(BF16)
             wsend_gu[e, rows, :, 128:256] = (ubuf[e, rows] * gain).astype(BF16)
 
@@ -135,6 +145,7 @@
     pl.semaphore_wait(barrier, NFS - 1 + 3)
     send_d(0)
 
+    loads[7].wait()
     r0, r1 = rt_ref[0:1, :], rt_ref[1:2, :]
     experts = lax.broadcasted_iota(jnp.int32, (64, 768), 0)
     oh0 = (experts == r0).astype(F32)
@@ -261,8 +272,6 @@
 
     def expert(e):
         got(wsend_gu.at[e, pl.ds(0, NFS - 1)], rwgu.at[e])
-        pltpu.make_async_copy(wgu.at[e, :, pl.ds(0, 128)], gate_out.at[e], out_sem.at[3 * e]).start()
-        pltpu.make_async_copy(wgu.at[e, :, pl.ds(128, 128)], up_out.at[e], out_sem.at[3 * e + 1]).start()
 
         def hrows(k):
             return pl.ds(pl.multiple_of(chunk_of(k) * CR, CR), CR)
@@ -319,7 +328,6 @@
         loop(NCH + 3, up_step)
 
         got(wsend_d.at[e, pl.ds(0, NFS - 1)], rwd.at[e])
-        pltpu.make_async_copy(wd.at[e], down_out.at[e], out_sem.at[3 * e + 2]).start()
 
         def send_r(k):
             plane = chunk_of(k) * 2
@@ -327,7 +335,7 @@
                 s = (plane + n // NY) * NY + (my + n) % NY
 
                 def go(s=s):
-                    remote(eo.at[e, s], ret.at[e, me], sr.at[e], rr.at[e], s, t).start()
+                    remote(eo.at[e, s], ret[e].at[me], sr.at[e], rr.at[e], s, t).start()
 
                 if n % NY == 0:
                     pl.when(s != me)(go)
@@ -353,13 +361,14 @@
                 send_r(k - 1)
 
         loop(NCH + 1, down_step)
-        ret[e, me] = eo[e, me]
+        ret[e][me] = eo[e, me]
 
     expert(0)
     expert(1)
 
     r0, r1 = rt_ref[0:1, :], rt_ref[1:2, :]
     rank0, rank1 = slots[0:1, :] - r0 * CAP, slots[1:2, :] - r1 * CAP
+    loads[8].wait()
     a0, a1 = at_ref[0:1, :], at_ref[1:2, :]
     total = a0 + a1
 
@@ -381,36 +390,44 @@
         for e in range(2):
             first = jnp.where(index == columns[:, 2 * e : 2 * e + 1], columns[:, 4:5], 0.0)
             second = jnp.where(index == columns[:, 2 * e + 1 : 2 * e + 2], columns[:, 5:6], 0.0)
-            wcomb[e, rows, :] = (first + second).astype(BF16)
+            wcomb[e][rows, :] = (first + second).astype(BF16)
 
     loop(12, weigh)
 
-    got(ret.at[0, pl.ds(0, NFS - 1)], rr.at[0])
+    got(ret0.at[pl.ds(0, NFS - 1)], rr.at[0])
 
     def mix_first(b):
         rows = pl.ds(pl.multiple_of(b * 256, 256), 256)
-        macc[rows, :] = jnp.dot(wcomb[0, rows, :], ret[0].reshape(NFS * CAP, 256), preferred_element_type=F32)
+        macc[rows, :] = jnp.dot(wcomb0[rows, :], ret0[...].reshape(NFS * CAP, 256), preferred_element_type=F32)
 
     loop(3, mix_first)
-    got(ret.at[1, pl.ds(0, NFS - 1)], rr.at[1])
-
-    def mix_second(b):
-        rows = pl.ds(pl.multiple_of(b * 256, 256), 256)
-        both = macc[rows, :] + jnp.dot(wcomb[1, rows, :], ret[1].reshape(NFS * CAP, 256), preferred_element_type=F32)
-        mixed_ref[rows, :] = both.astype(BF16)
-
-    loop(3, mix_second)
+    got(ret1.at[pl.ds(0, NFS - 1)], rr.at[1])
 
     for e in range(2):
         sent(wsend_gu.at[e, pl.ds(0, NFS - 1)], swgu.at[e])
         sent(wsend_d.at[e, pl.ds(0, NFS - 1)], swd.at[e])
         sent(hid.at[pl.ds(0, 7), e], sh.at[e])
         sent(eo.at[e, pl.ds(0, NFS - 1)], sr.at[e])
-        pltpu.make_async_copy(wgu.at[e, :, pl.ds(0, 128)], gate_out.at[e], out_sem.at[3 * e]).wait()
-        pltpu.make_async_copy(wgu.at[e, :, pl.ds(128, 128)], up_out.at[e], out_sem.at[3 * e + 1]).wait()
-        pltpu.make_async_copy(wd.at[e], down_out.at[e], out_sem.at[3 * e + 2]).wait()
     sent(outbox.at[pl.ds(0, 2 * (NFS - 1))], st)
     sent(tok.at[pl.ds(0, 7)], sx)
+
+
+def finish(wgu, wd, macc, wcomb1, ret1, mixed_out, gate_out, up_out, down_out, mixed, sem):
+    copies = [
+        pltpu.make_async_copy(wgu.at[:, :, pl.ds(0, 128)], gate_out, sem.at[0]),
+        pltpu.make_async_copy(wgu.at[:, :, pl.ds(128, 128)], up_out, sem.at[1]),
+        pltpu.make_async_copy(wd, down_out, sem.at[2]),
+    ]
+    for c in copies:
+        c.start()
+    for b in range(3):
+        rows = pl.ds(b * 256, 256)
+        odd = jnp.dot(wcomb1[rows, :], ret1[...].reshape(NFS * CAP, 256), preferred_element_type=F32)
+        mixed[rows, :] = (macc[rows, :] + odd).astype(BF16)
+    last = pltpu.make_async_copy(mixed, mixed_out, sem.at[3])
+    last.start()
+    for c in copies + [last]:
+        c.wait()
 
 
 def per_device(prompt, routes, affinity, norm_gain, gate_master, up_master, down_master):
@@ -418,6 +435,9 @@
     hbm = pl.BlockSpec(memory_space=pl.ANY)
     dma = pltpu.SemaphoreType.DMA
     scratch = [
+        pltpu.VMEM((2, 768), jnp.int32),
+        pltpu.VMEM((2, 768), F32),
+        pltpu.VMEM((1, 64), F32),
         pltpu.VMEM((768, 2048), BF16),
         pltpu.VMEM((2, 32, 64, 128), F32),
         pltpu.VMEM((2, 32, 64, 128), F32),
@@ -427,16 +447,12 @@
         pltpu.VMEM((768, 256), BF16),
         pltpu.VMEM((64, CAP, 256), BF16),
         pltpu.VMEM((NTP, NFS, 2, CAP, 256), BF16),
-        pltpu.VMEM((2, 2048, 256), BF16),
-        pltpu.VMEM((2, 1024, 256), BF16),
         pltpu.VMEM((NTP, 2, NFS * CAP, 128), BF16),
         pltpu.VMEM((2, NFS, CAP, 256), BF16),
-        pltpu.VMEM((2, NFS, CAP, 256), BF16),
-        pltpu.VMEM((2, 768, NFS * CAP), BF16),
-        pltpu.VMEM((768, 256), F32),
+        pltpu.VMEM((NFS, CAP, 256), BF16),
+        pltpu.VMEM((768, NFS * CAP), BF16),
         pltpu.VMEM((8, 768), jnp.int32),
-        dma((7,)),
-        dma((6,)),
+        dma((10,)),
         dma((2,)), dma((2,)), dma((2,)), dma((2,)),
         dma, dma,
         *[dma((NZ,)) for _ in range(9)],
@@ -444,30 +460,45 @@
         *[dma((2, 4)) for _ in range(8)],
         dma((2,)), dma((2,)),
     ]
+    landed = pl.pallas_call(
+        kernel,
+        out_shape=(
+            pltpu.VMEM((2, 2048, 256), BF16),
+            pltpu.VMEM((2, 1024, 256), BF16),
+            pltpu.VMEM((768, 256), F32),
+            pltpu.VMEM((768, NFS * CAP), BF16),
+            pltpu.VMEM((NFS, CAP, 256), BF16),
+        ),
+        in_specs=[hbm] * 7,
+        out_specs=(vmem,) * 5,
+        scratch_shapes=scratch,
+        compiler_params=pltpu.CompilerParams(
+            collective_id=0, has_side_effects=True, vmem_limit_bytes=50 * 1024 * 1024
+        ),
+        name="hand_off",
+    )(
+        routes.T,
+        affinity.T,
+        norm_gain.reshape(1, 64),
+        prompt,
+        gate_master.reshape(32, 2, 64, 128),
+        up_master.reshape(32, 2, 64, 128),
+        down_master.reshape(32, 2, 32, 256),
+    )
     return pl.pallas_call(
-        kernel,
+        finish,
         out_shape=(
             jax.ShapeDtypeStruct((768, 256), BF16),
             jax.ShapeDtypeStruct((2, 2048, 128), BF16),
             jax.ShapeDtypeStruct((2, 2048, 128), BF16),
             jax.ShapeDtypeStruct((2, 1024, 256), BF16),
         ),
-        in_specs=[vmem] * 3 + [hbm] * 4,
-        out_specs=(vmem, hbm, hbm, hbm),
-        scratch_shapes=scratch,
-        compiler_params=pltpu.CompilerParams(
-            collective_id=0, has_side_effects=True, vmem_limit_bytes=60 * 1024 * 1024
-        ),
-        name="hand_off",
-    )(
-        routes.T,
-        affinity.T,
-        jnp.broadcast_to(norm_gain[:, None], (64, 128)),
-        prompt,
-        gate_master.reshape(32, 2, 64, 128),
-        up_master.reshape(32, 2, 64, 128),
-        down_master.reshape(32, 2, 32, 256),
-    )
+        in_specs=[vmem] * 5,
+        out_specs=(hbm,) * 4,
+        scratch_shapes=[pltpu.VMEM((768, 256), BF16), dma((4,))],
+        compiler_params=pltpu.CompilerParams(vmem_limit_bytes=8 * 1024 * 1024),
+        name="finish",
+    )(*landed)
 
 
 def solution(mesh):

time: 159 us -> 151 us (0.950)
  local copies, waits for them, and re-layouts: 7.5 us -> 0 us
    unnamed x8 -> x0, local copies, waits for them, and re-layouts: 6.15 us -> none
    pallas_call x1 -> x2, Pallas kernels: 150 us -> 150 us  [the longest x1 148 us: per_device(): pl.pallas_call(kernel, out_shape=(pltpu.VMEM((2, 2048, 256), BF16), pltpu...]
where the time goes in v3:
time: 151 us; the launch traced here: 150 us
  Pallas kernels  150 us (99%)
    pallas_call x1, Pallas kernels, per_device(): pl.pallas_call(kernel, out_shape=(pltpu.VMEM((2, 2048, 256), BF16), pltpu...  148 us

profile of v3, /device:TPU:32, one launch (start us, length us, event | category | flops | bytes accessed | tf_op | source)
XLA Modules:
  0.0 150.4 jit_solution(15371782498346271930)
XLA Ops:
  0.6 147.9 %hand_off.1 = (bf16[2,2048,256]{2,1,0:T(8,128)(2,1)S(1)}, bf16[2,1024,256]{2,1,0:T(8,128)(2,1)S(1)}, f32[768,256]{1,0:T(8,128)S(1)}, bf16[768,1536]{1,0:T(8,128)(2,1)S(1)}, bf16[32,48,256]{2,1,0:T(8,128)(2,1)S(1)}) custom-call(s32[2,768]{1,0:T(2,128)} %bitcast.9, f32[2,768]{1,0:T(2,128)} %bitcast.10, f32[1,64]{1,0:T(1,128)} %bitcast.11, ...), custom_call_target="tpu_custom_call" | custom-call | tf_op jit(solution)/shard_map/hand_off/pallas_call | solution.py:463
  148.5 1.8 %finish.1 = (bf16[768,256]{1,0:T(8,128)(2,1)}, bf16[2,2048,128]{2,1,0:T(8,128)(2,1)}, bf16[2,2048,128]{2,1,0:T(8,128)(2,1)}, bf16[2,1024,256]{2,1,0:T(8,128)(2,1)}) custom-call(bf16[2,2048,256]{2,1,0:T(8,128)(2,1)S(1)} %get-tuple-element.9.wgu, bf16[2,1024,256]{2,1,0:T(8,128)(2,1)S(1)} %get-tuple-element.10.wd, f32[768,256]{1,0:T(8,128)S(1)} %get-tuple-element.11.macc, ...), custom_call_target="tpu_custom_call" | custom-call | tf_op jit(solution)/shard_map/finish/pallas_call | solution.py:488

commit v4 on v3

--- a/solution.py
+++ b/solution.py
@@ -19,19 +19,19 @@
     return NZ + ((i + 1) // 2) * (2 * (i % 2) - 1)
 
 
-def loop(count, body):
+def loop(count, body, start=0):
     def step(i, carry):
         body(i)
         return carry
 
-    lax.fori_loop(0, count, step, 0)
+    lax.fori_loop(start, count, step, 0)
 
 
 def kernel(
     rt_hbm, at_hbm, gain_hbm, prompt_ref, gate_ref, up_ref, down_ref,
     wgu, wd, macc, wcomb1, ret1,
-    rt_ref, at_ref, gain_ref, pbuf, gbuf, ubuf, dbuf, wsend_gu, wsend_d, nm, outbox, tok, hid, eo, ret0, wcomb0,
-    slots, load_sem, swgu, swd, rwgu, rwd, st, sx, own, xl, xr, fl, fr, po, pl_, pr, pf,
+    rt_ref, at_ref, gain_ref, pbuf, gbuf, ubuf, dbuf, wsend_gu, wsend_d, nm, blk, near, outbox, tok, hid, eo, ret0, wcomb0,
+    slots, load_sem, sa, rblk, rnear, swgu, swd, rwgu, rwd, st, sx, own, xl, xr, fl, fr, po, pl_, pr, pf,
     sh, hxl, hxr, hfl, hfr, hpo, hpl, hpr, hpf, sr, rr,
 ):
     me = lax.axis_index("fs")
@@ -60,7 +60,7 @@
         load(8, at_hbm, at_ref),
         load(9, gain_hbm, gain_ref),
     ]
-    for n in (0, 7, 1, 9, 2, 3, 4, 5, 6, 8):
+    for n in (1, 7, 0, 9, 2, 3, 4, 5, 6, 8):
         loads[n].start()
 
     barrier = pltpu.get_barrier_semaphore()
@@ -83,7 +83,7 @@
     def sent(ref, sem):
         remote(ref, ref, sem, sem, me, t).wait_send()
 
-    def to_peers(send):
+    def to_peers(send, first=0, last=NZ):
         def plane(i):
             z = (mz + plane_step(i)) % NZ
             for dy in range(NY):
@@ -95,7 +95,7 @@
                 else:
                     send(dst)
 
-        loop(NZ, plane)
+        loop(last, plane, first)
 
     def cast_gu(e):
         if e == 0:
@@ -133,17 +133,28 @@
         loop(8, block)
         wd[e, pl.ds(pl.multiple_of(me * 32, 32), 32), :] = wsend_d[e, me]
 
-    def send_d(e):
+    def send_d(e, first=0, last=NZ):
         def send(dst):
             remote(
                 wsend_d.at[e, dst], wd.at[e, pl.ds(pl.multiple_of(me * 32, 32), 32)], swd.at[e], rwd.at[e], dst, t
             ).start()
 
-        to_peers(send)
-
-    cast_d(0)
+        to_peers(send, first, last)
+
+    loads[1].wait()
+
+    def norm(b):
+        rows = pl.ds(pl.multiple_of(b * 64, 64), 64)
+        x = pbuf[rows, :].astype(F32)
+        scale = lax.rsqrt(jnp.mean(x * x, axis=-1, keepdims=True) + norm_eps)
+        mine = pbuf[rows, pl.ds(pl.multiple_of(t * 256, 256), 256)].astype(F32)
+        nm[rows, :] = (mine * scale).astype(BF16)
+
+    loop(12, norm)
+    above, below = (mz + 1) % NZ * NY + my, (mz + NZ - 1) % NZ * NY + my
     pl.semaphore_wait(barrier, NFS - 1 + 3)
-    send_d(0)
+    remote(nm, blk.at[0], sa.at[0], rblk.at[0], above, t).start()
+    remote(nm, blk.at[1], sa.at[0], rblk.at[1], below, t).start()
 
     loads[7].wait()
     r0, r1 = rt_ref[0:1, :], rt_ref[1:2, :]
@@ -154,56 +165,31 @@
     count = jnp.dot((oh0 + oh1).astype(BF16), before.astype(F32).astype(BF16), preferred_element_type=F32)
     rank0 = jnp.sum(count * oh0, axis=0, keepdims=True).astype(jnp.int32)
     rank1 = jnp.sum(count * oh1, axis=0, keepdims=True).astype(jnp.int32)
-    slots[0:1, :] = r0 * CAP + rank0
-    slots[1:2, :] = r1 * CAP + rank1
-
-    loads[1].wait()
-
-    def norm(b):
-        rows = pl.ds(pl.multiple_of(b * 64, 64), 64)
-        x = pbuf[rows, :].astype(F32)
-        scale = lax.rsqrt(jnp.mean(x * x, axis=-1, keepdims=True) + norm_eps)
-        mine = pbuf[rows, pl.ds(pl.multiple_of(t * 256, 256), 256)].astype(F32)
-        nm[rows, :] = (mine * scale).astype(BF16)
-
-    loop(12, norm)
-
-    def build(i):
-        z = (mz + plane_step(i)) % NZ
+    slots[...] = jnp.concatenate([r0 * CAP + rank0, r1 * CAP + rank1, jnp.zeros((6, 768), jnp.int32)], axis=0)
+
+    def pack(block, s0, s1, index):
+        hit = (index == s0) | (index == s1)
+        rows = jnp.dot(hit.astype(F32).astype(BF16), block, preferred_element_type=F32)
+        return rows.astype(BF16)
+
+    def pack_plane(block, s0, s1, z):
         index = lax.broadcasted_iota(jnp.int32, (8 * CAP, 768), 0) + z * (8 * CAP)
-        hit = (index == slots[0:1, :]) | (index == slots[1:2, :])
-        rows = jnp.dot(hit.astype(F32).astype(BF16), nm[...], preferred_element_type=F32)
-        outbox[pl.ds(z * 8, 8)] = rows.astype(BF16).reshape(8, CAP, 256)
-
-    def send_t(i):
-        z = (mz + plane_step(i)) % NZ
-        for dy in range(NY):
-            dst = z * NY + (my + dy) % NY
-
-            def go(dst=dst):
-                remote(outbox.at[pl.ds(dst * 2, 2)], tok.at[t, me], st, own.at[i], dst, t).start()
-
-            if dy == 0:
-                pl.when(i > 0)(go)
-            else:
-                go()
-
-    def dispatch(i):
-        build(i)
-
-        @pl.when(i > 0)
-        def _():
-            send_t(i - 1)
-
-    loop(NZ, dispatch)
-    tok[t, me] = outbox[pl.ds(me * 2, 2)]
-    cast_gu(0)
-    send_t(NZ - 1)
-    send_gu(0)
-    cast_gu(1)
-    cast_d(1)
-    send_gu(1)
-    send_d(1)
+        return pack(block, s0, s1, index).reshape(8, CAP, 256)
+
+    def pack_half(block, s0, s1, z, e):
+        turn = lax.broadcasted_iota(jnp.int32, (4, CAP, 768), 0) * (2 * CAP)
+        index = turn + lax.broadcasted_iota(jnp.int32, (4, CAP, 768), 1) + (z * (8 * CAP) + e * CAP)
+        return pack(block, s0, s1, index.reshape(4 * CAP, 768)).reshape(4, CAP, 256)
+
+    outbox[0:8] = pack_plane(nm[...], slots[0:1, :], slots[1:2, :], mz)
+    remote(slots, near.at[0], sa.at[1], rnear.at[0], above, t).start()
+    remote(slots, near.at[1], sa.at[1], rnear.at[1], below, t).start()
+    tok[t, me] = outbox[pl.ds(my * 2, 2)]
+    cast_d(0)
+    for dy in range(1, NY):
+        y = (my + dy) % NY
+        remote(outbox.at[pl.ds(y * 2, 2)], tok.at[t, me], st, own.at[0], mz * NY + y, t).start()
+    send_d(0, 0, 5)
 
     def plane_rows(i):
         z = (mz + 2 * NZ - plane_step(i)) % NZ
@@ -214,11 +200,11 @@
         def _():
             at = plane_rows(i)
 
-            @pl.when(i > 0)
+            @pl.when(i > 2)
             def _():
                 got(tok.at[t, pl.ds(at, NY)], own.at[i])
 
-            @pl.when(i == 0)
+            @pl.when(i <= 2)
             def _():
                 got(tok.at[t, pl.ds(at, NY - 1)], own.at[i])
 
@@ -251,7 +237,61 @@
             got(tok.at[far, pl.ds(at + NY // 2, NY // 2)], fr.at[j])
             remote(whole, whole, sx, pf.at[j], me, mate).start()
 
-    loop(NZ + 2, gather)
+    def side_of(d, side):
+        way = 1 - 2 * side
+        return (mz + NZ - way) % NZ * NY + my, (mz + NZ + way * (d - 1)) % NZ
+
+    def build(d):
+        def one(side):
+            src, z = side_of(d, side)
+            s0, s1 = near[side, 0:1, :], near[side, 1:2, :]
+            base = 8 + (side * 4 + d - 1) * 8
+            if d < 4:
+                outbox[pl.ds(base, 8)] = pack_plane(blk[side], s0, s1, z)
+            else:
+                outbox[pl.ds(base, 4)] = pack_half(blk[side], s0, s1, z, side)
+            if d == 1:
+                tok[t, src] = outbox[pl.ds(base + my * 2, 2)]
+
+        loop(2, one)
+
+    def relay(d):
+        def one(side):
+            src, z = side_of(d, side)
+            base = 8 + (side * 4 + d - 1) * 8
+            group = 7 if d == 4 else 2 * d - 1 + side
+            for dy in range(1 if d == 1 else 0, NY):
+                y = (my + dy) % NY
+                if d < 4:
+                    remote(outbox.at[pl.ds(base + y * 2, 2)], tok.at[t, src], st, own.at[group], z * NY + y, t).start()
+                else:
+                    remote(outbox.at[base + y], tok.at[t, src, side], st, own.at[group], z * NY + y, t).start()
+
+        loop(2, one)
+
+    loop(1, gather)
+    for side in range(2):
+        got(near.at[side], rnear.at[side])
+        got(blk.at[side], rblk.at[side])
+    build(2)
+    relay(2)
+    build(1)
+    relay(1)
+    build(3)
+    relay(3)
+    loop(2, gather, 1)
+    build(4)
+    relay(4)
+    loop(3, gather, 2)
+    cast_gu(0)
+    send_d(0, 5, NZ)
+    send_gu(0)
+    loop(4, gather, 3)
+    cast_gu(1)
+    cast_d(1)
+    send_gu(1)
+    send_d(1)
+    loop(NZ + 2, gather, 4)
 
     def gathered(i):
         at = pl.ds(plane_rows(i), NY)
@@ -408,7 +448,9 @@
         sent(wsend_d.at[e, pl.ds(0, NFS - 1)], swd.at[e])
         sent(hid.at[pl.ds(0, 7), e], sh.at[e])
         sent(eo.at[e, pl.ds(0, NFS - 1)], sr.at[e])
-    sent(outbox.at[pl.ds(0, 2 * (NFS - 1))], st)
+    sent(outbox.at[pl.ds(0, 58)], st)
+    sent(blk, sa.at[0])
+    sent(near, sa.at[1])
     sent(tok.at[pl.ds(0, 7)], sx)
 
 
@@ -445,7 +487,9 @@
         pltpu.VMEM((2, 32, 64, 256), BF16),
         pltpu.VMEM((2, 32, 32, 256), BF16),
         pltpu.VMEM((768, 256), BF16),
-        pltpu.VMEM((64, CAP, 256), BF16),
+        pltpu.VMEM((2, 768, 256), BF16),
+        pltpu.VMEM((2, 8, 768), jnp.int32),
+        pltpu.VMEM((9 * 8, CAP, 256), BF16),
         pltpu.VMEM((NTP, NFS, 2, CAP, 256), BF16),
         pltpu.VMEM((NTP, 2, NFS * CAP, 128), BF16),
         pltpu.VMEM((2, NFS, CAP, 256), BF16),
@@ -453,6 +497,7 @@
         pltpu.VMEM((768, NFS * CAP), BF16),
         pltpu.VMEM((8, 768), jnp.int32),
         dma((10,)),
+        dma((2,)), dma((2,)), dma((2,)),
         dma((2,)), dma((2,)), dma((2,)), dma((2,)),
         dma, dma,
         *[dma((NZ,)) for _ in range(9)],

time: 151 us -> 146 us (0.967)
  Pallas kernels: 150 us -> 145 us
    pallas_call x1, Pallas kernels: 148 us -> 143 us  [per_device(): pl.pallas_call(kernel, out_shape=(pltpu.VMEM((2, 2048, 256), BF16), pltpu...]
where the time goes in v4:
time: 146 us
  Pallas kernels  145 us (99%)
    pallas_call x1, Pallas kernels, per_device(): pl.pallas_call(kernel, out_shape=(pltpu.VMEM((2, 2048, 256), BF16), pltpu...  143 us

profile of v4, /device:TPU:32, one launch (start us, length us, event | category | flops | bytes accessed | tf_op | source)
XLA Modules:
  0.0 145.6 jit_solution(11729485486889002620)
XLA Ops:
  0.6 143.1 %hand_off.1 = (bf16[2,2048,256]{2,1,0:T(8,128)(2,1)S(1)}, bf16[2,1024,256]{2,1,0:T(8,128)(2,1)S(1)}, f32[768,256]{1,0:T(8,128)S(1)}, bf16[768,1536]{1,0:T(8,128)(2,1)S(1)}, bf16[32,48,256]{2,1,0:T(8,128)(2,1)S(1)}) custom-call(s32[2,768]{1,0:T(2,128)} %bitcast.9, f32[2,768]{1,0:T(2,128)} %bitcast.10, f32[1,64]{1,0:T(1,128)} %bitcast.11, ...), custom_call_target="tpu_custom_call" | custom-call | tf_op jit(solution)/shard_map/hand_off/pallas_call | solution.py:508
  143.7 1.8 %finish.1 = (bf16[768,256]{1,0:T(8,128)(2,1)}, bf16[2,2048,128]{2,1,0:T(8,128)(2,1)}, bf16[2,2048,128]{2,1,0:T(8,128)(2,1)}, bf16[2,1024,256]{2,1,0:T(8,128)(2,1)}) custom-call(bf16[2,2048,256]{2,1,0:T(8,128)(2,1)S(1)} %get-tuple-element.9.wgu, bf16[2,1024,256]{2,1,0:T(8,128)(2,1)S(1)} %get-tuple-element.10.wd, f32[768,256]{1,0:T(8,128)S(1)} %get-tuple-element.11.macc, ...), custom_call_target="tpu_custom_call" | custom-call | tf_op jit(solution)/shard_map/finish/pallas_call | solution.py:533

commit v5 on v4

--- a/solution.py
+++ b/solution.py
@@ -60,7 +60,7 @@
         load(8, at_hbm, at_ref),
         load(9, gain_hbm, gain_ref),
     ]
-    for n in (1, 7, 0, 9, 2, 3, 4, 5, 6, 8):
+    for n in (0, 1, 7, 9, 2, 3, 4, 5, 6, 8):
         loads[n].start()
 
     barrier = pltpu.get_barrier_semaphore()
@@ -115,13 +115,13 @@
         loop(8, block)
         wgu[e, pl.ds(pl.multiple_of(me * 64, 64), 64), :] = wsend_gu[e, me]
 
-    def send_gu(e):
+    def send_gu(e, first=0, last=NZ):
         def send(dst):
             remote(
                 wsend_gu.at[e, dst], wgu.at[e, pl.ds(pl.multiple_of(me * 64, 64), 64)], swgu.at[e], rwgu.at[e], dst, t
             ).start()
 
-        to_peers(send)
+        to_peers(send, first, last)
 
     def cast_d(e):
         loads[0 if e == 0 else 6].wait()
@@ -140,6 +140,10 @@
             ).start()
 
         to_peers(send, first, last)
+
+    cast_d(0)
+    pl.semaphore_wait(barrier, NFS - 1 + 3)
+    send_d(0, 0, 5)
 
     loads[1].wait()
 
@@ -152,7 +156,6 @@
 
     loop(12, norm)
     above, below = (mz + 1) % NZ * NY + my, (mz + NZ - 1) % NZ * NY + my
-    pl.semaphore_wait(barrier, NFS - 1 + 3)
     remote(nm, blk.at[0], sa.at[0], rblk.at[0], above, t).start()
     remote(nm, blk.at[1], sa.at[0], rblk.at[1], below, t).start()
 
@@ -165,7 +168,7 @@
     count = jnp.dot((oh0 + oh1).astype(BF16), before.astype(F32).astype(BF16), preferred_element_type=F32)
     rank0 = jnp.sum(count * oh0, axis=0, keepdims=True).astype(jnp.int32)
     rank1 = jnp.sum(count * oh1, axis=0, keepdims=True).astype(jnp.int32)
-    slots[...] = jnp.concatenate([r0 * CAP + rank0, r1 * CAP + rank1, jnp.zeros((6, 768), jnp.int32)], axis=0)
+    slots[...] = jnp.concatenate([r0 * CAP + rank0, r1 * CAP + rank1], axis=0)
 
     def pack(block, s0, s1, index):
         hit = (index == s0) | (index == s1)
@@ -184,12 +187,13 @@
     outbox[0:8] = pack_plane(nm[...], slots[0:1, :], slots[1:2, :], mz)
     remote(slots, near.at[0], sa.at[1], rnear.at[0], above, t).start()
     remote(slots, near.at[1], sa.at[1], rnear.at[1], below, t).start()
+    remote(slots, near.at[2], sa.at[1], rnear.at[2], (mz + 2) % NZ * NY + my, t).start()
+    remote(slots, near.at[3], sa.at[1], rnear.at[3], (mz + NZ - 2) % NZ * NY + my, t).start()
     tok[t, me] = outbox[pl.ds(my * 2, 2)]
-    cast_d(0)
     for dy in range(1, NY):
         y = (my + dy) % NY
         remote(outbox.at[pl.ds(y * 2, 2)], tok.at[t, me], st, own.at[0], mz * NY + y, t).start()
-    send_d(0, 0, 5)
+    send_d(0, 5, 7)
 
     def plane_rows(i):
         z = (mz + 2 * NZ - plane_step(i)) % NZ
@@ -200,11 +204,11 @@
         def _():
             at = plane_rows(i)
 
-            @pl.when(i > 2)
+            @pl.when(i > 4)
             def _():
                 got(tok.at[t, pl.ds(at, NY)], own.at[i])
 
-            @pl.when(i <= 2)
+            @pl.when(i <= 4)
             def _():
                 got(tok.at[t, pl.ds(at, NY - 1)], own.at[i])
 
@@ -239,28 +243,30 @@
 
     def side_of(d, side):
         way = 1 - 2 * side
-        return (mz + NZ - way) % NZ * NY + my, (mz + NZ + way * (d - 1)) % NZ
+        dist = min(d, 2)
+        held = side + 2 * (dist - 1)
+        return held, (mz + NZ - way * dist) % NZ * NY + my, (mz + NZ + way * (d - dist)) % NZ
 
     def build(d):
         def one(side):
-            src, z = side_of(d, side)
-            s0, s1 = near[side, 0:1, :], near[side, 1:2, :]
+            held, src, z = side_of(d, side)
+            s0, s1 = near[held, 0:1, :], near[held, 1:2, :]
             base = 8 + (side * 4 + d - 1) * 8
             if d < 4:
-                outbox[pl.ds(base, 8)] = pack_plane(blk[side], s0, s1, z)
+                outbox[pl.ds(base, 8)] = pack_plane(blk[held], s0, s1, z)
             else:
-                outbox[pl.ds(base, 4)] = pack_half(blk[side], s0, s1, z, side)
-            if d == 1:
+                outbox[pl.ds(base, 4)] = pack_half(blk[held], s0, s1, z, side)
+            if d <= 2:
                 tok[t, src] = outbox[pl.ds(base + my * 2, 2)]
 
         loop(2, one)
 
     def relay(d):
         def one(side):
-            src, z = side_of(d, side)
+            held, src, z = side_of(d, side)
             base = 8 + (side * 4 + d - 1) * 8
             group = 7 if d == 4 else 2 * d - 1 + side
-            for dy in range(1 if d == 1 else 0, NY):
+            for dy in range(1 if d <= 2 else 0, NY):
                 y = (my + dy) % NY
                 if d < 4:
                     remote(outbox.at[pl.ds(base + y * 2, 2)], tok.at[t, src], st, own.at[group], z * NY + y, t).start()
@@ -273,25 +279,30 @@
     for side in range(2):
         got(near.at[side], rnear.at[side])
         got(blk.at[side], rblk.at[side])
+        remote(blk.at[side], blk.at[2 + side], sa.at[0], rblk.at[2 + side], below if side else above, t).start()
+    build(1)
+    relay(1)
+    send_d(0, 7, NZ)
+    cast_gu(0)
+    send_gu(0, 0, 5)
+    loop(2, gather, 1)
+    for side in range(2, 4):
+        got(near.at[side], rnear.at[side])
+        got(blk.at[side], rblk.at[side])
     build(2)
     relay(2)
-    build(1)
-    relay(1)
     build(3)
     relay(3)
-    loop(2, gather, 1)
+    loop(3, gather, 2)
     build(4)
     relay(4)
-    loop(3, gather, 2)
-    cast_gu(0)
-    send_d(0, 5, NZ)
-    send_gu(0)
+    send_gu(0, 5, NZ)
+    cast_gu(1)
+    send_gu(1)
     loop(4, gather, 3)
-    cast_gu(1)
     cast_d(1)
-    send_gu(1)
     send_d(1)
-    loop(NZ + 2, gather, 4)
+    loop(NZ, gather, 4)
 
     def gathered(i):
         at = pl.ds(plane_rows(i), NY)
@@ -300,21 +311,22 @@
         got(tok.at[right + 1 - 2 * mc, at], pr.at[i])
         got(tok.at[far + 1 - 2 * mc, at], pf.at[i])
 
-    loop(NZ, gathered)
 
     CH = 8
     NCH = NFS // CH
     CR = CH * CAP
 
-    def chunk_of(k):
-        step = (2 + ((k + 1) // 2) * (1 - 2 * (k % 2))) % NCH
+    def chunk_of(k, e):
+        if e == 0:
+            step = ((k + 1) % 3 + 1) * ((k + 3) // 4)
+        else:
+            step = 2 + ((k + 1) // 2) * (1 - 2 * (k % 2))
         return (mz // 2 + step) % NCH
 
-    def expert(e):
-        got(wsend_gu.at[e, pl.ds(0, NFS - 1)], rwgu.at[e])
+    def phases(e):
 
         def hrows(k):
-            return pl.ds(pl.multiple_of(chunk_of(k) * CR, CR), CR)
+            return pl.ds(pl.multiple_of(chunk_of(k, e) * CR, CR), CR)
 
         def send_h(k):
             piece = hid.at[t, e, hrows(k)]
@@ -323,7 +335,7 @@
             remote(piece, piece, sh.at[e], hpo.at[e, k], me, mate).start()
 
         def forward_h(k):
-            base = pl.multiple_of(chunk_of(k) * CR, CR)
+            base = pl.multiple_of(chunk_of(k, e) * CR, CR)
             whole = hid.at[left, e, pl.ds(base, CR)]
             half = hid.at[left, e, pl.ds(base, CR // 2)]
             got(whole, hxl.at[e, k])
@@ -336,41 +348,37 @@
             remote(whole, whole, sh.at[e], hpr.at[e, k], me, mate).start()
 
         def pass_h(k):
-            base = pl.multiple_of(chunk_of(k) * CR, CR)
+            base = pl.multiple_of(chunk_of(k, e) * CR, CR)
             whole = hid.at[far, e, pl.ds(base, CR)]
             got(hid.at[far, e, pl.ds(base, CR // 2)], hfl.at[e, k])
             got(hid.at[far, e, pl.ds(base + CR // 2, CR // 2)], hfr.at[e, k])
             remote(whole, whole, sh.at[e], hpf.at[e, k], me, mate).start()
 
-        def up_step(k):
-            @pl.when(k < NCH)
-            def _():
-                senders = pl.ds(chunk_of(k) * CH, CH)
-                acc = jnp.zeros((CR, 256), F32)
-                for p in range(NTP):
-                    x = tok[p, senders, e].reshape(CR, 256)
-                    acc = acc + jnp.dot(x, wgu[e, p * 256 : (p + 1) * 256, :], preferred_element_type=F32)
-                gate, up = acc[:, 0:128], acc[:, 128:256]
-                hid[t, e, hrows(k), :] = (gate / (1.0 + jnp.exp(-gate)) * up).astype(BF16)
-
-            @pl.when((k >= 1) & (k < NCH + 1))
-            def _():
-                send_h(k - 1)
-
-            @pl.when((k >= 2) & (k < NCH + 2))
-            def _():
-                forward_h(k - 2)
-
-            @pl.when(k >= 3)
-            def _():
-                pass_h(k - 3)
-
-        loop(NCH + 3, up_step)
-
-        got(wsend_d.at[e, pl.ds(0, NFS - 1)], rwd.at[e])
+        def compute_h(k):
+            senders = pl.ds(chunk_of(k, e) * CH, CH)
+            acc = jnp.zeros((CR, 256), F32)
+            for p in range(NTP):
+                x = tok[p, senders, e].reshape(CR, 256)
+                acc = acc + jnp.dot(x, wgu[e, p * 256 : (p + 1) * 256, :], preferred_element_type=F32)
+            gate, up = acc[:, 0:128], acc[:, 128:256]
+            hid[t, e, hrows(k), :] = (gate / (1.0 + jnp.exp(-gate)) * up).astype(BF16)
+
+        def hidden(first, last):
+            def step(k):
+                pl.when(k < NCH)(lambda: compute_h(k))
+                pl.when(k >= 1)(lambda: send_h(k - 1))
+
+            loop(last, step, first)
+
+        def forwarding():
+            def step(k):
+                pl.when(k < NCH)(lambda: forward_h(k))
+                pl.when(k >= 1)(lambda: pass_h(k - 1))
+
+            loop(NCH + 1, step)
 
         def send_r(k):
-            plane = chunk_of(k) * 2
+            plane = chunk_of(k, e) * 2
             for n in range(CH):
                 s = (plane + n // NY) * NY + (my + n) % NY
 
@@ -394,17 +402,38 @@
                 for q in range(NX):
                     h = jnp.concatenate([hid[2 * q, e, rows, :], hid[2 * q + 1, e, rows, :]], axis=1)
                     acc = acc + jnp.dot(h, wd[e, q * 256 : (q + 1) * 256, :], preferred_element_type=F32)
-                eo[e, pl.ds(chunk_of(k) * CH, CH)] = acc.astype(BF16).reshape(CH, CAP, 256)
+                eo[e, pl.ds(chunk_of(k, e) * CH, CH)] = acc.astype(BF16).reshape(CH, CAP, 256)
 
             @pl.when(k >= 1)
             def _():
                 send_r(k - 1)
 
-        loop(NCH + 1, down_step)
-        ret[e][me] = eo[e, me]
-
-    expert(0)
-    expert(1)
+        def returns():
+            got(wsend_d.at[e, pl.ds(0, NFS - 1)], rwd.at[e])
+            loop(NCH + 1, down_step)
+            ret[e][me] = eo[e, me]
+
+        return hidden, forwarding, returns
+
+    hidden_even, forwarding_even, returns_even = phases(0)
+    hidden_odd, forwarding_odd, returns_odd = phases(1)
+    loop(NZ + 1, gather, NZ)
+    loop(3, gathered)
+    got(wsend_gu.at[0, pl.ds(0, NFS - 1)], rwgu.at[0])
+    hidden_even(0, 1)
+    loop(NZ + 2, gather, NZ + 1)
+    loop(6, gathered, 3)
+    hidden_even(1, 2)
+    loop(7, gathered, 6)
+    hidden_even(2, 3)
+    loop(NZ, gathered, 7)
+    hidden_even(3, NCH + 1)
+    forwarding_even()
+    got(wsend_gu.at[1, pl.ds(0, NFS - 1)], rwgu.at[1])
+    hidden_odd(0, NCH + 1)
+    returns_even()
+    forwarding_odd()
+    returns_odd()
 
     r0, r1 = rt_ref[0:1, :], rt_ref[1:2, :]
     rank0, rank1 = slots[0:1, :] - r0 * CAP, slots[1:2, :] - r1 * CAP
@@ -448,7 +477,7 @@
         sent(wsend_d.at[e, pl.ds(0, NFS - 1)], swd.at[e])
         sent(hid.at[pl.ds(0, 7), e], sh.at[e])
         sent(eo.at[e, pl.ds(0, NFS - 1)], sr.at[e])
-    sent(outbox.at[pl.ds(0, 58)], st)
+    sent(outbox.at[pl.ds(0, 54)], st)
     sent(blk, sa.at[0])
     sent(near, sa.at[1])
     sent(tok.at[pl.ds(0, 7)], sx)
@@ -487,17 +516,17 @@
         pltpu.VMEM((2, 32, 64, 256), BF16),
         pltpu.VMEM((2, 32, 32, 256), BF16),
         pltpu.VMEM((768, 256), BF16),
-        pltpu.VMEM((2, 768, 256), BF16),
-        pltpu.VMEM((2, 8, 768), jnp.int32),
+        pltpu.VMEM((4, 768, 256), BF16),
+        pltpu.VMEM((4, 2, 768), jnp.int32),
         pltpu.VMEM((9 * 8, CAP, 256), BF16),
         pltpu.VMEM((NTP, NFS, 2, CAP, 256), BF16),
         pltpu.VMEM((NTP, 2, NFS * CAP, 128), BF16),
         pltpu.VMEM((2, NFS, CAP, 256), BF16),
         pltpu.VMEM((NFS, CAP, 256), BF16),
         pltpu.VMEM((768, NFS * CAP), BF16),
-        pltpu.VMEM((8, 768), jnp.int32),
+        pltpu.VMEM((2, 768), jnp.int32),
         dma((10,)),
-        dma((2,)), dma((2,)), dma((2,)),
+        dma((2,)), dma((4,)), dma((4,)),
         dma((2,)), dma((2,)), dma((2,)), dma((2,)),
         dma, dma,
         *[dma((NZ,)) for _ in range(9)],

time: 146 us -> 144 us (0.986)
  Pallas kernels: 145 us -> 143 us
    pallas_call x1, Pallas kernels: 143 us -> 141 us  [per_device(): pl.pallas_call(kernel, out_shape=(pltpu.VMEM((2, 2048, 256), BF16), pltpu...]
where the time goes in v5:
time: 144 us
  Pallas kernels  143 us (99%)
    pallas_call x1, Pallas kernels, per_device(): pl.pallas_call(kernel, out_shape=(pltpu.VMEM((2, 2048, 256), BF16), pltpu...  141 us

profile of v5, /device:TPU:32, one launch (start us, length us, event | category | flops | bytes accessed | tf_op | source)
XLA Modules:
  0.0 143.9 jit_solution(14046878020375072827)
XLA Ops:
  0.6 141.5 %hand_off.1 = (bf16[2,2048,256]{2,1,0:T(8,128)(2,1)S(1)}, bf16[2,1024,256]{2,1,0:T(8,128)(2,1)S(1)}, f32[768,256]{1,0:T(8,128)S(1)}, bf16[768,1536]{1,0:T(8,128)(2,1)S(1)}, bf16[32,48,256]{2,1,0:T(8,128)(2,1)S(1)}) custom-call(s32[2,768]{1,0:T(2,128)} %bitcast.9, f32[2,768]{1,0:T(2,128)} %bitcast.10, f32[1,64]{1,0:T(1,128)} %bitcast.11, ...), custom_call_target="tpu_custom_call" | custom-call | tf_op jit(solution)/shard_map/hand_off/pallas_call | solution.py:537
  142.1 1.8 %finish.1 = (bf16[768,256]{1,0:T(8,128)(2,1)}, bf16[2,2048,128]{2,1,0:T(8,128)(2,1)}, bf16[2,2048,128]{2,1,0:T(8,128)(2,1)}, bf16[2,1024,256]{2,1,0:T(8,128)(2,1)}) custom-call(bf16[2,2048,256]{2,1,0:T(8,128)(2,1)S(1)} %get-tuple-element.9.wgu, bf16[2,1024,256]{2,1,0:T(8,128)(2,1)S(1)} %get-tuple-element.10.wd, f32[768,256]{1,0:T(8,128)S(1)} %get-tuple-element.11.macc, ...), custom_call_target="tpu_custom_call" | custom-call | tf_op jit(solution)/shard_map/finish/pallas_call | solution.py:562

commit v6 on v5

--- a/solution.py
+++ b/solution.py
@@ -143,7 +143,7 @@
 
     cast_d(0)
     pl.semaphore_wait(barrier, NFS - 1 + 3)
-    send_d(0, 0, 5)
+    send_d(0, 0, 3)
 
     loads[1].wait()
 
@@ -193,7 +193,7 @@
     for dy in range(1, NY):
         y = (my + dy) % NY
         remote(outbox.at[pl.ds(y * 2, 2)], tok.at[t, me], st, own.at[0], mz * NY + y, t).start()
-    send_d(0, 5, 7)
+    send_d(0, 3, 5)
 
     def plane_rows(i):
         z = (mz + 2 * NZ - plane_step(i)) % NZ
@@ -282,9 +282,9 @@
         remote(blk.at[side], blk.at[2 + side], sa.at[0], rblk.at[2 + side], below if side else above, t).start()
     build(1)
     relay(1)
-    send_d(0, 7, NZ)
+    send_d(0, 5, NZ)
     cast_gu(0)
-    send_gu(0, 0, 5)
+    send_gu(0, 0, 3)
     loop(2, gather, 1)
     for side in range(2, 4):
         got(near.at[side], rnear.at[side])
@@ -296,7 +296,7 @@
     loop(3, gather, 2)
     build(4)
     relay(4)
-    send_gu(0, 5, NZ)
+    send_gu(0, 3, NZ)
     cast_gu(1)
     send_gu(1)
     loop(4, gather, 3)

time: 144 us -> 143 us (level)
  no operation moved by 1% of the time
where the time goes in v6:
time: 143 us
  Pallas kernels  142 us (99%)
    pallas_call x1, Pallas kernels, per_device(): pl.pallas_call(kernel, out_shape=(pltpu.VMEM((2, 2048, 256), BF16), pltpu...  140 us

profile of v6, /device:TPU:32, one launch (start us, length us, event | category | flops | bytes accessed | tf_op | source)
XLA Modules:
  0.0 142.9 jit_solution(16743701949411240539)
XLA Ops:
  0.6 140.4 %hand_off.1 = (bf16[2,2048,256]{2,1,0:T(8,128)(2,1)S(1)}, bf16[2,1024,256]{2,1,0:T(8,128)(2,1)S(1)}, f32[768,256]{1,0:T(8,128)S(1)}, bf16[768,1536]{1,0:T(8,128)(2,1)S(1)}, bf16[32,48,256]{2,1,0:T(8,128)(2,1)S(1)}) custom-call(s32[2,768]{1,0:T(2,128)} %bitcast.9, f32[2,768]{1,0:T(2,128)} %bitcast.10, f32[1,64]{1,0:T(1,128)} %bitcast.11, ...), custom_call_target="tpu_custom_call" | custom-call | tf_op jit(solution)/shard_map/hand_off/pallas_call | solution.py:537
  141.0 1.8 %finish.1 = (bf16[768,256]{1,0:T(8,128)(2,1)}, bf16[2,2048,128]{2,1,0:T(8,128)(2,1)}, bf16[2,2048,128]{2,1,0:T(8,128)(2,1)}, bf16[2,1024,256]{2,1,0:T(8,128)(2,1)}) custom-call(bf16[2,2048,256]{2,1,0:T(8,128)(2,1)S(1)} %get-tuple-element.9.wgu, bf16[2,1024,256]{2,1,0:T(8,128)(2,1)S(1)} %get-tuple-element.10.wd, f32[768,256]{1,0:T(8,128)S(1)} %get-tuple-element.11.macc, ...), custom_call_target="tpu_custom_call" | custom-call | tf_op jit(solution)/shard_map/finish/pallas_call | solution.py:562
